TPU v7x, 512 devices: a whole 4x8x8 slice. The times are simulated.
512 devices in a mesh: dp: 4 (over x), kv: 64 (over z, y), tp: 2 (over core).
Axes of the slice: x: 4, y: 8, z: 8, core: 2. Of those that a mesh axis runs over, the one named last changes fastest.
Arguments:
- tokens: bfloat16 [512, 2048], P('dp', 'kv'), may hold values from -16 to 16
- pre_gain: float32 [2048], P('kv'), may hold values from 0.1 to 1.9
- query_weight: bfloat16 [2048, 1024], P('kv', 'tp'), may hold values from -0.125 to 0.125
- key_weight: bfloat16 [2048, 1024], P('kv', 'tp'), may hold values from -0.125 to 0.125
- value_weight: bfloat16 [2048, 1024], P('kv', 'tp'), may hold values from -0.125 to 0.125
- outgate_weight: bfloat16 [2048, 1024], P('kv', 'tp'), may hold values from -0.125 to 0.125
- input_gate_weight: bfloat16 [2048, 4], replicated, may hold values from -0.125 to 0.125
- forget_gate_weight: bfloat16 [2048, 4], replicated, may hold values from -0.125 to 0.125
- cache_keys: bfloat16 [512, 64, 1024], P(('dp', 'kv'), None, 'tp'), may hold values from -6 to 6
- cache_values: bfloat16 [512, 64, 1024], P(('dp', 'kv'), None, 'tp'), may hold values from -6 to 6
- cache_input: float32 [512, 64, 4], P(('dp', 'kv'), None, 'tp'), may hold values from -6 to 250
- cache_forget: float32 [512, 64, 4], P(('dp', 'kv'), None, 'tp'), may hold values from -0.7 to 0
- lengths: int32 [512], P(('dp', 'kv')), may hold values from 1 to 64, 13107 in all
- state_matrix: float32 [512, 4, 256, 256], P(('dp', 'kv'), 'tp'), may hold values from -6 to 6
- state_norm: float32 [512, 4, 256], P(('dp', 'kv'), 'tp'), may hold values from -6 to 6
- state_max: float32 [512, 4], P(('dp', 'kv'), 'tp'), may hold values from -4 to 253
- head_gain: float32 [1024], P('tp'), may hold values from 0.1 to 1.9
- out_weight: bfloat16 [1024, 2048], P('tp', 'kv'), may hold values from -0.375 to 0.375
- mixer_gain: float32 [2048], replicated, may hold values from 0.1 to 1.9
- gate_weight: bfloat16 [2048, 5632], P(None, ('kv', 'tp')), may hold values from -0.125 to 0.125
- up_weight: bfloat16 [2048, 5632], P(None, ('kv', 'tp')), may hold values from -0.125 to 0.125
- down_weight: bfloat16 [5632, 2048], P(('kv', 'tp')), may hold values from -0.625 to 0.625
Outputs:
- layer_out: bfloat16 [512, 2048], P('dp', ('kv', 'tp'))
Inputs may be any that keep to these rules, and one draw needn't show every extreme that they name: `lengths`: positions from a sequence's length on take no part.
All inputs are finite; a program needn't handle non-finite values. No bound on the sum of `lengths` on one device may be relied on, other than what follows from the above.
Results may differ from a plain program's by a relative error of at most 0.018.
Values may be sent and summed in bfloat16 or wider, within the bound.
A program may use at most 64 MiB of HBM per device.

v0:
```python
import math

import jax
import jax.numpy as jnp
from jax import lax
from jax.sharding import Mesh
from jax.sharding import PartitionSpec as P

KV = ("kv_0", "kv_1")
KV_TP = ("kv_0", "kv_1", "tp")
DP_KV = ("dp", "kv_0", "kv_1")


EPS = 1e-06


def in_blocks(shard, dim, length):
    before, after = (shard.shape[:dim], shard.shape[dim + 1 :])
    return jnp.moveaxis(shard.reshape(*before, length, -1, *after), dim, 0)


def sum_at_owner(shard, axis, dim):
    length = lax.axis_size(axis)
    pieces = lax.all_to_all(in_blocks(shard, dim, length), axis, 0, 0, tiled=True)
    return jnp.sum(pieces.astype(jnp.float32), axis=0)


def in_one_piece(arrays, axis, dim, along):
    widths = [math.prod(a.shape[along:]) for a in arrays]
    both = jnp.concatenate(
        [a.reshape(*a.shape[:along], w) for a, w in zip(arrays, widths)], axis=along
    )
    filled = sum_at_owner(both, axis, dim)
    pieces = jnp.split(filled, [sum(widths[:k]) for k in range(1, len(widths))], axis=along)
    return tuple(
        (b.reshape(*filled.shape[:along], *a.shape[along:]) for a, b in zip(arrays, pieces))
    )


def laid_out(pieces, dim):
    lengths = list(pieces.shape[1:])
    lengths[dim] *= pieces.shape[0]
    return jnp.moveaxis(pieces, 0, dim).reshape(lengths)


def from_everyone(shard, axis):
    copies = jnp.broadcast_to(shard, (lax.axis_size(axis), *shard.shape))
    return lax.all_to_all(copies, axis, split_axis=0, concat_axis=0, tiled=True)


def gather_directly(shard, axis, dim):
    return laid_out(from_everyone(shard, axis), dim)


def gather_axes(shard, axes, dim):
    far, near = axes
    pieces = from_everyone(from_everyone(shard, far), near)
    return laid_out(pieces.swapaxes(0, 1).reshape(-1, *shard.shape), dim)


def per_device(
    tokens,
    pre_gain,
    query_weight,
    key_weight,
    value_weight,
    outgate_weight,
    input_gate_weight,
    forget_gate_weight,
    cache_keys,
    cache_values,
    cache_input,
    cache_forget,
    lengths,
    state_matrix,
    state_norm,
    state_max,
    head_gain,
    out_weight,
    mixer_gain,
    gate_weight,
    up_weight,
    down_weight,
):
    col_width = tokens.shape[1]
    own_seqs = cache_keys.shape[0]
    block_len = cache_keys.shape[1]
    head_count = state_max.shape[1]
    head_size = state_norm.shape[2]
    shard_index = lax.axis_index(KV)
    half_index = lax.axis_index("tp")
    kv_count = lax.axis_size(KV)
    tp_count = lax.axis_size("tp")
    model_width = col_width * kv_count
    token_values = tokens.astype(jnp.float32)
    squares = jnp.sum(token_values * token_values, axis=1)
    normed = (token_values * pre_gain[None, :]).astype(jnp.bfloat16)
    corner = (shard_index * col_width, half_index * head_count)
    gate_pair = jnp.concatenate(
        [
            lax.dynamic_slice(input_gate_weight, corner, (col_width, head_count)),
            lax.dynamic_slice(forget_gate_weight, corner, (col_width, head_count)),
        ],
        axis=1,
    )

    def product(weight):
        return jnp.dot(normed, weight, preferred_element_type=jnp.float32)

    query_term = product(query_weight)
    key_term = product(key_weight)
    value_term = product(value_weight)
    outgate_term = product(outgate_weight)
    gate_term = product(gate_pair)
    query_sum, key_sum, value_sum, outgate_sum, gate_sum, own_squares = in_one_piece(
        (
            query_term.astype(jnp.bfloat16),
            key_term.astype(jnp.bfloat16),
            value_term.astype(jnp.bfloat16),
            outgate_term.astype(jnp.bfloat16),
            gate_term.astype(jnp.bfloat16),
            squares.astype(jnp.bfloat16),
        ),
        KV,
        0,
        1,
    )
    scale_first = lax.rsqrt(own_squares / model_width + EPS)[:, None]
    query = (scale_first * query_sum).astype(jnp.bfloat16)
    keys_new = (scale_first * key_sum).astype(jnp.bfloat16)
    values_new = (scale_first * value_sum).astype(jnp.bfloat16)
    outgate = (scale_first * outgate_sum).astype(jnp.bfloat16)
    gate_values = scale_first * gate_sum
    in_gate = gate_values[:, :head_count]
    forget_new = jax.nn.log_sigmoid(gate_values[:, head_count:])
    query_heads = query.reshape(own_seqs, head_count, head_size)
    key_heads = keys_new.reshape(own_seqs, head_count, head_size)
    value_heads = values_new.reshape(own_seqs, head_count, head_size)
    cached_keys = cache_keys.reshape(own_seqs, block_len, head_count, head_size)
    cached_values = cache_values.reshape(own_seqs, block_len, head_count, head_size)
    inv_root = head_size ** (-0.5)
    live_mask = (lax.broadcasted_iota(jnp.int32, (own_seqs, block_len), 1) < lengths[:, None])[
        :, :, None
    ]
    forget_live = jnp.where(live_mask, cache_forget, jnp.float32(0.0))
    running = jnp.cumsum(forget_live, axis=1)
    total_log = running[:, -1, :] + forget_new
    weight_log = jnp.where(live_mask, total_log[:, None, :] - running + cache_input, -jnp.inf)
    state_log = total_log + state_max
    peak_log = jnp.maximum(jnp.maximum(state_log, in_gate), jnp.max(weight_log, axis=1))
    key_dots = (
        jnp.einsum("shd,slhd->slh", query_heads, cached_keys, preferred_element_type=jnp.float32)
        * inv_root
    )
    block_scores = jnp.exp(weight_log - peak_log[:, None, :]) * key_dots
    query_scaled = query_heads.astype(jnp.float32) * inv_root
    self_score = jnp.exp(in_gate - peak_log) * jnp.sum(
        query_scaled * key_heads.astype(jnp.float32), axis=2
    )
    carried = jnp.exp(state_log - peak_log)
    block_weights = block_scores.astype(jnp.bfloat16)
    memory_read = jnp.einsum(
        "shvd,shd->shv", state_matrix, query_scaled, precision=lax.Precision.HIGHEST
    )
    norm_read = jnp.einsum("shd,shd->sh", state_norm, query_scaled, precision=lax.Precision.HIGHEST)
    numerator = (
        carried[:, :, None] * memory_read
        + jnp.einsum(
            "slh,slhd->shd", block_weights, cached_values, preferred_element_type=jnp.float32
        )
        + self_score[:, :, None] * value_heads.astype(jnp.float32)
    )
    denominator = carried * norm_read + jnp.sum(block_scores, axis=1) + self_score
    hidden = numerator / jnp.maximum(jnp.abs(denominator), 1.0)[:, :, None]
    mixed_heads = (
        hidden.reshape(own_seqs, head_count * head_size)
        * head_gain[None, :]
        * jax.nn.sigmoid(outgate.astype(jnp.float32))
    ).astype(jnp.bfloat16)
    mix_terms = jnp.dot(
        gather_directly(mixed_heads, KV, 0), out_weight, preferred_element_type=jnp.float32
    )
    mix_sum = sum_at_owner(mix_terms.astype(jnp.bfloat16), "tp", 1)
    narrow = mix_sum.shape[1]
    residual = (
        lax.dynamic_slice_in_dim(token_values, half_index * narrow, narrow, 1) + mix_sum
    ).astype(jnp.bfloat16)
    hidden_cols = gate_weight.shape[1]
    piece_wide = gather_axes(residual, (("kv_0", "kv_1"), "tp"), 1).astype(jnp.float32)
    normed_piece = (piece_wide * mixer_gain[None, :]).astype(jnp.bfloat16)
    gate_acc = jnp.dot(normed_piece, gate_weight, preferred_element_type=jnp.float32)
    up_acc = jnp.dot(normed_piece, up_weight, preferred_element_type=jnp.float32)
    sum_squares = jnp.sum(piece_wide * piece_wide, axis=1)
    gate_acc, up_acc, sum_squares = (gate_acc, up_acc, sum_squares)
    scale_mid = lax.rsqrt(sum_squares / model_width + EPS)[:, None]
    hidden_units = (jax.nn.silu(scale_mid * gate_acc) * (scale_mid * up_acc)).astype(jnp.bfloat16)
    block_width = model_width // (kv_count * tp_count)
    half_rows = kv_count * block_width
    down_grid = down_weight.reshape(hidden_cols, kv_count, tp_count * block_width)
    offset = jnp.int32(0)
    count_rows = half_rows * lax.axis_size("tp")
    pieces = []
    for step_half in range(count_rows // half_rows):
        which_half = offset // half_rows + step_half
        columns = lax.dynamic_slice_in_dim(
            down_grid, which_half * block_width, block_width, 2
        ).reshape(hidden_cols, half_rows)
        pieces.append(
            lax.dot_general(
                columns, hidden_units, (((0,), (1,)), ((), ())), preferred_element_type=jnp.float32
            )
        )
    core_total = sum_at_owner(jnp.concatenate(pieces, axis=0).astype(jnp.bfloat16), "tp", 0)
    summed = sum_at_owner(core_total.astype(jnp.bfloat16), KV, 0)
    mixer_out = summed.T
    return (residual.astype(jnp.float32) + mixer_out).astype(jnp.bfloat16)


def solution(mesh):
    split = Mesh(
        mesh.devices.reshape(mesh.shape["dp"], 8, 8, mesh.shape["tp"]), ("dp", "kv_0", "kv_1", "tp")
    )
    return jax.shard_map(
        per_device,
        mesh=split,
        in_specs=(
            P("dp", KV),
            P(KV),
            P(KV, "tp"),
            P(KV, "tp"),
            P(KV, "tp"),
            P(KV, "tp"),
            P(),
            P(),
            P(DP_KV, None, "tp"),
            P(DP_KV, None, "tp"),
            P(DP_KV, None, "tp"),
            P(DP_KV, None, "tp"),
            P(DP_KV),
            P(DP_KV, "tp", None, None),
            P(DP_KV, "tp", None),
            P(DP_KV, "tp"),
            P("tp"),
            P("tp", KV),
            P(),
            P(None, KV_TP),
            P(None, KV_TP),
            P(KV_TP, None),
        ),
        out_specs=P("dp", KV_TP),
        check_vma=False,
    )
```

profile of v0, /device:TPU:1, one launch (start us, length us, event | category | flops | bytes accessed | tf_op | source)
XLA Modules:
  0.0 123.4 jit_solution(9736044306903035107)
XLA Ops:
  0.0 0.8 dynamic_slice.16
  0.9 0.8 dynamic_slice.17
  1.6 0.7 multiply_reduce_fusion.1
  2.4 0.9 convolution_convert_fusion.7
  3.3 0.1 copy.78
  3.4 0.2 convert_element_type.170
  3.6 1.1 convolution_convert_fusion.5
  4.8 1.1 convolution_convert_fusion.4
  5.9 0.3 convolution_convert_fusion.3
  6.3 0.3 convolution_convert_fusion.2
  6.7 3.0 %concatenate.27 = bf16[64,2,2053]{2,1,0:T(2,128)(2,1)} concatenate(bf16[64,2,512]{2,1,0:T(2,128)(2,1)S(1)} %concatenate.21, bf16[64,2,512]{2,1,0:T(2,128)(2,1)S(1)} %concatenate.22, bf16[64,2,512]{2,1,0:T(2,128)(2,1)S(1)} %concatenate.23, bf16[64,2,512]{2,1,0:T(2,128)(2,1)S(1)} %concatenate.24, bf16[64,2,4]{2,1,0:T(2,128)(2,1)S(1)} %bitcast.86, ...), dimensions={2} | concatenate | bytes 1051136 | tf_op jit(solution)/shard_map/concatenate | solution.py:30
  9.7 17.3 %all-to-all-start = ((bf16[64,2,2053]{2,1,0:T(2,128)(2,1)}), bf16[64,2,2053]{2,1,0:T(2,128)(2,1)S(1)}, u32[]{:S(2)}, u32[]{:S(2)}) async-start(bf16[64,2,2053]{2,1,0:T(2,128)(2,1)} %concatenate.27), calls=%async_computation | async-start | bytes 1114112 | tf_op jit(solution)/shard_map/all_to_all | solution.py:24
  27.1 0.1 copy.77
  27.2 0.1 reduce_window_sum.11
  27.4 17.1 %all-to-all-done = bf16[64,2,2053]{2,1,0:T(2,128)(2,1)S(1)} async-done(((bf16[64,2,2053]{2,1,0:T(2,128)(2,1)}), bf16[64,2,2053]{2,1,0:T(2,128)(2,1)S(1)}, u32[]{:S(2)}, u32[]{:S(2)}) %all-to-all-start) | async-done | bytes 525600 | tf_op jit(solution)/shard_map/all_to_all | solution.py:24
  44.6 0.5 convert_reduce_fusion
  45.0 0.2 fusion.33
  45.5 0.2 fusion.35
  45.7 0.1 fusion.8
  45.8 0.2 fusion.36
  46.0 0.1 fusion.5
  46.3 1.0 fusion.18
  47.4 0.7 broadcast_in_dim.46
  48.2 7.2 %all-to-all-start.1 = ((bf16[64,2,512]{2,1,0:T(2,128)(2,1)}), bf16[64,2,512]{2,1,0:T(2,128)(2,1)S(1)}, u32[]{:S(2)}, u32[]{:S(2)}) async-start(bf16[64,2,512]{2,1,0:T(2,128)(2,1)} %broadcast_in_dim.46), calls=%async_computation.1 | async-start | bytes 262144 | tf_op jit(solution)/shard_map/all_to_all | solution.py:48
  55.3 11.5 %all-to-all-done.1 = bf16[64,2,512]{2,1,0:T(2,128)(2,1)S(1)} async-done(((bf16[64,2,512]{2,1,0:T(2,128)(2,1)}), bf16[64,2,512]{2,1,0:T(2,128)(2,1)S(1)}, u32[]{:S(2)}, u32[]{:S(2)}) %all-to-all-start.1) | async-done | bytes 131104 | tf_op jit(solution)/shard_map/all_to_all | solution.py:48
  66.9 0.1 convolution_convert_fusion.6
  67.1 6.3 %all_to_all.35 = bf16[2,128,16]{1,2,0:T(8,128)(2,1)S(1)} all-to-all(bf16[2,128,16]{1,2,0:T(8,128)(2,1)S(1)} %bitcast.88), channel_id=1, replica_groups=mesh['dp'=4,'kv_0'=8,'kv_1'=8,'tp'=2] {'tp'}, dimensions={0} | all-to-all | bytes 16384 | tf_op jit(solution)/shard_map/all_to_all | solution.py:24
  73.4 0.7 broadcast_in_dim.47
  74.1 4.6 %all-to-all-start.3 = ((bf16[64,128,16]{1,2,0:T(8,128)(2,1)}), bf16[64,128,16]{1,2,0:T(8,128)(2,1)S(1)}, u32[]{:S(2)}, u32[]{:S(2)}) async-start(bf16[64,128,16]{1,2,0:T(8,128)(2,1)} %broadcast_in_dim.47), calls=%async_computation.3 | async-start | bytes 524288 | tf_op jit(solution)/shard_map/all_to_all | solution.py:48
  78.7 0.5 reshape.106
  79.2 0.3 fusion.37
  79.6 0.9 copy.82
  80.5 0.9 copy.83
  81.4 10.8 %all-to-all-done.3 = bf16[64,128,16]{1,2,0:T(8,128)(2,1)S(1)} async-done(((bf16[64,128,16]{1,2,0:T(8,128)(2,1)}), bf16[64,128,16]{1,2,0:T(8,128)(2,1)S(1)}, u32[]{:S(2)}, u32[]{:S(2)}) %all-to-all-start.3) | async-done | bytes 262176 | tf_op jit(solution)/shard_map/all_to_all | solution.py:48
  92.3 6.1 %all_to_all.36 = bf16[2,64,128,16]{2,3,1,0:T(8,128)(2,1)S(1)} all-to-all(bf16[2,64,128,16]{2,3,1,0:T(8,128)(2,1)S(1)} %broadcast_in_dim.48), channel_id=1, replica_groups=mesh['dp'=4,'kv_0'=8,'kv_1'=8,'tp'=2] {'tp'}, dimensions={0} | all-to-all | bytes 1048576 | tf_op jit(solution)/shard_map/all_to_all | solution.py:48
  98.4 0.3 multiply_reduce_fusion
  98.7 0.1 copy_convert_fusion
  98.9 0.3 copy-done.9
  99.1 0.3 fusion.4
  99.5 0.6 copy-done.3
  100.1 0.2 convolution_multiply_fusion.1
  100.3 0.2 fusion.3
  100.5 0.2 fusion
  100.8 0.2 fusion.1
  101.1 4.2 %all_to_all.37 = bf16[2,1024,128]{1,2,0:T(8,128)(2,1)S(1)} all-to-all(bf16[2,1024,128]{1,2,0:T(8,128)(2,1)S(1)} %bitcast.82), channel_id=1, replica_groups=mesh['dp'=4,'kv_0'=8,'kv_1'=8,'tp'=2] {'tp'}, dimensions={0} | all-to-all | bytes 1048576 | tf_op jit(solution)/shard_map/all_to_all | solution.py:24
  105.4 0.2 copy.86
  105.5 17.2 %all_to_all.38 = bf16[64,16,128]{2,1,0:T(8,128)(2,1)S(1)} all-to-all(bf16[64,16,128]{2,1,0:T(8,128)(2,1)S(1)} %bitcast.83), channel_id=1, replica_groups=mesh['dp'=4,'kv_0'=8,'kv_1'=8,'tp'=2] {'kv_0','kv_1'}, dimensions={0} | all-to-all | bytes 524288 | tf_op jit(solution)/shard_map/all_to_all | solution.py:24
  122.8 0.6 fusion.11
  (65 shorter events, 1.4 us)
Async XLA Ops:
  0.0 46.3 %copy-start = (f32[2,2,256,256]{3,2,1,0:T(8,128)S(1)}, f32[2,2,256,256]{3,2,1,0:T(8,128)}, u32[]{:S(2)}) copy-start(f32[2,2,256,256]{3,2,1,0:T(8,128)} %param.35) | copy-start | bytes 3145732
  0.0 5.9 %copy-start.1 = (bf16[128,32]{0,1:T(8,128)(2,1)S(1)}, bf16[128,32]{0,1:T(8,128)(2,1)}, u32[]{:S(2)}) copy-start(bf16[128,32]{0,1:T(8,128)(2,1)} %param.22) | copy-start | bytes 24580
  0.0 5.9 %copy-start.10 = (f32[32]{0:T(128)S(1)}, f32[32]{0:T(128)}, u32[]{:S(2)}) copy-start(f32[32]{0:T(128)} %param.23) | copy-start | bytes 388
  0.0 5.9 %copy-start.6 = (bf16[32,512]{1,0:T(8,128)(2,1)S(1)}, bf16[32,512]{1,0:T(8,128)(2,1)}, u32[]{:S(2)}) copy-start(bf16[32,512]{1,0:T(8,128)(2,1)} %param.26) | copy-start | bytes 98308
  0.0 6.3 %copy-start.7 = (bf16[32,512]{1,0:T(8,128)(2,1)S(1)}, bf16[32,512]{1,0:T(8,128)(2,1)}, u32[]{:S(2)}) copy-start(bf16[32,512]{1,0:T(8,128)(2,1)} %param.27) | copy-start | bytes 98308
  6.7 20.4 %copy-start.17 = (s32[2]{0:T(128)S(1)}, s32[2]{0:T(128)}, u32[]{:S(2)}) copy-start(s32[2]{0:T(128)} %param.34) | copy-start | bytes 28
  6.7 20.4 %copy-start.14 = (f32[2,64,2]{1,2,0:T(2,128)S(1)}, f32[2,64,2]{1,2,0:T(2,128)}, u32[]{:S(2)}) copy-start(f32[2,64,2]{1,2,0:T(2,128)} %param.33) | copy-start | bytes 3076
  9.7 35.8 %copy-start.11 = (f32[2,64,2]{1,2,0:T(2,128)S(1)}, f32[2,64,2]{1,2,0:T(2,128)}, u32[]{:S(2)}) copy-start(f32[2,64,2]{1,2,0:T(2,128)} %param.32) | copy-start | bytes 3076
  9.7 36.0 %copy-start.15 = (f32[2,2]{1,0:T(2,128)S(1)}, f32[2,2]{1,0:T(2,128)}, u32[]{:S(2)}) copy-start(f32[2,2]{1,0:T(2,128)} %param.37) | copy-start | bytes 52
  9.7 36.0 %copy-start.16 = (bf16[2,64,512]{2,1,0:T(8,128)(2,1)S(1)}, bf16[2,64,512]{2,1,0:T(8,128)(2,1)}, u32[]{:S(2)}) copy-start(bf16[2,64,512]{2,1,0:T(8,128)(2,1)} %param.30) | copy-start | bytes 393220
  9.7 36.3 %copy-start.5 = (bf16[2,64,512]{2,1,0:T(8,128)(2,1)S(1)}, bf16[2,64,512]{2,1,0:T(8,128)(2,1)}, u32[]{:S(2)}) copy-start(bf16[2,64,512]{2,1,0:T(8,128)(2,1)} %param.31) | copy-start | bytes 393220
  9.7 36.4 %copy-start.12 = (f32[2,2,256]{2,1,0:T(2,128)S(1)}, f32[2,2,256]{2,1,0:T(2,128)}, u32[]{:S(2)}) copy-start(f32[2,2,256]{2,1,0:T(2,128)} %param.36) | copy-start | bytes 12292
  9.7 34.8 %all-to-all-start = ((bf16[64,2,2053]{2,1,0:T(2,128)(2,1)}), bf16[64,2,2053]{2,1,0:T(2,128)(2,1)S(1)}, u32[]{:S(2)}, u32[]{:S(2)}) async-start(bf16[64,2,2053]{2,1,0:T(2,128)(2,1)} %concatenate.27), calls=%async_computation | async-start | bytes 1114112 | tf_op jit(solution)/shard_map/all_to_all | solution.py:24
  27.4 19.9 %copy-start.13 = (f32[512]{0:T(512)S(1)}, f32[512]{0:T(512)}, u32[]{:S(2)}) copy-start(f32[512]{0:T(512)} %param.38) | copy-start | bytes 6148
  45.7 21.2 %copy-start.8 = (bf16[512,32]{0,1:T(8,128)(2,1)S(1)}, bf16[512,32]{0,1:T(8,128)(2,1)}, u32[]{:S(2)}) copy-start(bf16[512,32]{0,1:T(8,128)(2,1)} %param.39) | copy-start | bytes 98308
  47.2 31.5 %copy-start.2 = (bf16[44,2048]{1,0:T(8,128)(2,1)S(1)}, bf16[44,2048]{1,0:T(8,128)(2,1)}, u32[]{:S(2)}) copy-start(bf16[44,2048]{1,0:T(8,128)(2,1)} %param.43) | copy-start | bytes 540676
  48.2 18.7 %all-to-all-start.1 = ((bf16[64,2,512]{2,1,0:T(2,128)(2,1)}), bf16[64,2,512]{2,1,0:T(2,128)(2,1)S(1)}, u32[]{:S(2)}, u32[]{:S(2)}) async-start(bf16[64,2,512]{2,1,0:T(2,128)(2,1)} %broadcast_in_dim.46), calls=%async_computation.1 | async-start | bytes 262144 | tf_op jit(solution)/shard_map/all_to_all | solution.py:48
  74.1 18.1 %all-to-all-start.3 = ((bf16[64,128,16]{1,2,0:T(8,128)(2,1)}), bf16[64,128,16]{1,2,0:T(8,128)(2,1)S(1)}, u32[]{:S(2)}, u32[]{:S(2)}) async-start(bf16[64,128,16]{1,2,0:T(8,128)(2,1)} %broadcast_in_dim.47), calls=%async_computation.3 | async-start | bytes 524288 | tf_op jit(solution)/shard_map/all_to_all | solution.py:48
  98.4 0.7 copy-start.9
  99.1 0.9 copy-start.3
  99.1 1.1 copy-start.4
where the time goes:
time: 125 us; the launch traced here: 123 us
  waiting for transfers between devices  39.5 us (32%)
  blocking collectives  33.8 us (27%)
  starting transfers between devices  29 us (23%)
  local copies, waits for them, and re-layouts  10.9 us (9%)
  matrix products  5.88 us (5%)
  other arithmetic  3.99 us (3%)
    all_to_all x3, blocking collectives, sum_at_owner(): lax.all_to_all(in_blocks(shard, dim, length), axis, 0, 0, tiled=True)  27.6 us
    all_to_all x2, waiting for transfers between devices, from_everyone(): return lax.all_to_all(copies, axis, split_axis=0, concat_axis=0, tiled=True)  22.3 us
    all_to_all x1, starting transfers between devices, sum_at_owner(): lax.all_to_all(in_blocks(shard, dim, length), axis, 0, 0, tiled=True)  17.3 us
    all_to_all x1, waiting for transfers between devices, sum_at_owner(): lax.all_to_all(in_blocks(shard, dim, length), axis, 0, 0, tiled=True)  17.1 us
    all_to_all x2, starting transfers between devices, from_everyone(): return lax.all_to_all(copies, axis, split_axis=0, concat_axis=0, tiled=True)  11.8 us
    all_to_all x1, blocking collectives, from_everyone(): return lax.all_to_all(copies, axis, split_axis=0, concat_axis=0, tiled=True)  6.13 us
    dot_general x5, matrix products, product(): return jnp.dot(normed, weight, preferred_element_type=jnp.float32)  3.6 us
    concatenate x5, local copies, waits for them, and re-layouts, in_one_piece(): jnp.concatenate([a.reshape(*a.shape[:along], w) for a, w in zip(arrays, w...  3.28 us
  transfers between devices with their start and end apart: 3, of which 3 were waited for; matrix products, arithmetic and copies ran while one was open for 2% of the time, Pallas kernels for 0%

commit v1 on v0

v1 whole, which is shorter than its diff:
```python
import functools

import jax
import jax.numpy as jnp
from jax import lax
from jax.experimental import pallas as pl
from jax.experimental.pallas import tpu as pltpu
from jax.sharding import PartitionSpec as P

EPS = 1e-06
MESH = pl.DeviceIdType.MESH
F32 = jnp.float32
BF16 = jnp.bfloat16
KINDS = 4
ROWS = 40
HIDDEN_PAD = 48


def ring_order(n):
    return sorted(range(1, n), key=lambda d: (-min(d, n - d), d))


def dot(a, b, ca=1, cb=0, precision=None):
    return lax.dot_general(
        a, b, (((ca,), (cb,)), ((), ())), preferred_element_type=F32, precision=precision
    )


def iota(shape, dim):
    return lax.broadcasted_iota(jnp.int32, shape, dim)


def kernel(
    n,
    tok_h,
    pre_h,
    qw_h,
    kw_h,
    vw_h,
    ow_h,
    ig_h,
    fg_h,
    ck_h,
    cv_h,
    ci_h,
    cf_h,
    len_h,
    sm_h,
    sn_h,
    smax_h,
    hg_h,
    mixw_h,
    mg_h,
    gw_h,
    uw_h,
    dw_h,
    out_ref,
    tok,
    pre,
    w4,
    gates,
    ck,
    cv,
    ci,
    cf,
    lens,
    state,
    sn,
    smax,
    hg,
    mixw,
    mg,
    gw,
    uw,
    dw,
    load_sem,
    p1,
    r1,
    q2f,
    q2b,
    r2,
    split,
    pick,
    mh,
    xs,
    xr,
    rbuf,
    rt,
    gu,
    dt,
    xo,
    xi,
    p5,
    p5b,
    r3,
    q4b,
    r4,
    s1,
    v1,
    s2,
    v2,
    s3,
    v3,
    s4,
    v4,
    s5,
    v5,
    s6,
    v6,
    s7,
    v7,
    s8,
    v8,
    s9,
    v9,
):
    kvs = n * n
    width = tok.shape[0]
    seqs = tok.shape[1]
    cols = w4.shape[2]
    blocks = cols // 128
    model = width * kvs
    dp = lax.axis_index("dp")
    kv = lax.axis_index("kv")
    tp = lax.axis_index("tp")
    z, y = kv // n, kv % n
    far = n - (n - 1) * tp
    near = 1 + (n - 1) * tp
    first = z + (y - z) * tp
    second = y + (z - y) * tp
    other = 1 - tp
    order = ring_order(n)

    def first_peer(d):
        return (dp, lax.rem(first + d, n) * far + second * near, tp)

    def second_peer(d):
        return (dp, first * far + lax.rem(second + d, n) * near, tp)

    sibling = (dp, kv, other)

    barrier = pltpu.get_barrier_semaphore()
    for d in range(1, n):
        pl.semaphore_signal(barrier, inc=1, device_id=first_peer(d), device_id_type=MESH)
        pl.semaphore_signal(barrier, inc=1, device_id=second_peer(d), device_id_type=MESH)
    pl.semaphore_signal(barrier, inc=1, device_id=sibling, device_id_type=MESH)

    loads = [
        (tok_h, tok),
        (pre_h, pre),
        (qw_h, w4.at[0]),
        (kw_h, w4.at[1]),
        (vw_h, w4.at[2]),
        (ow_h, w4.at[3]),
        (ig_h, gates.at[0]),
        (fg_h, gates.at[1]),
        (cf_h, cf),
        (ci_h, ci),
        (len_h, lens),
        (smax_h, smax),
        (sm_h, state),
        (sn_h, sn),
        (ck_h, ck),
        (cv_h, cv),
        (hg_h, hg),
        (mixw_h, mixw),
        (mg_h, mg),
        (gw_h, gw),
        (uw_h, uw),
        (dw_h, dw),
    ]
    copies = [pltpu.make_async_copy(a, b, load_sem.at[k]) for k, (a, b) in enumerate(loads)]
    for c in copies:
        c.start()
    for c in copies[:8]:
        c.wait()

    r = iota((seqs, seqs), 0)
    owner = (r // (2 * n)) * far + (r % n) * near
    perm = jnp.where(iota((seqs, seqs), 1) == owner * 2 + (r // n) % 2, 1.0, 0.0).astype(BF16)
    tokens = dot(perm, tok[...], 1, 1)
    squares = jnp.sum(tokens * tokens, axis=1, keepdims=True)
    normed = (tokens * pre[...]).astype(BF16)
    for k in range(KINDS):
        prod = dot(normed, w4[k]).astype(BF16)
        p1[:, :, k * cols : (k + 1) * cols] = prod.reshape(n, 2 * n, cols)
    lane0 = pl.multiple_of((kv // (128 // width)) * 128, 128)
    both = jnp.concatenate(
        [gates[0, :, pl.ds(lane0, 128)].astype(F32), gates[1, :, pl.ds(lane0, 128)].astype(F32)],
        axis=0,
    ).astype(BF16)
    at = (kv % (128 // width)) * width
    sel = jnp.where(iota((width, 128), 1) == iota((width, 128), 0) + at, 1.0, 0.0).astype(BF16)
    own_gates = dot(both, sel, 1, 1)
    own_gates = jnp.concatenate([own_gates, jnp.zeros((120, width), F32)], axis=0).astype(BF16)
    g = dot(normed, own_gates, 1, 1)
    g = jnp.where(iota((seqs, 128), 1) == 8, squares, g)
    p1[:, :, KINDS * cols :] = g.astype(BF16).reshape(n, 2 * n, 128)

    pl.semaphore_wait(barrier, 2 * (n - 1) + 1)

    def exchange(src, dst, send, recv, peer):
        made = {}
        for d in order:
            made[d] = pltpu.make_async_remote_copy(
                src_ref=src(d),
                dst_ref=dst(d),
                send_sem=send.at[d - 1],
                recv_sem=recv.at[d - 1],
                device_id=peer(d),
                device_id_type=MESH,
            )
            made[d].start()
        return made

    one = exchange(
        lambda d: p1.at[lax.rem(first + d, n)], lambda d: r1.at[d - 1], s1, v1, first_peer
    )

    for c in copies[8:]:
        c.wait()
    row64 = iota((8, ck.shape[1]), 0)
    lane64 = iota((8, ck.shape[1]), 1)
    zero4 = jnp.zeros((4, ck.shape[1]), F32)
    forget = jnp.concatenate([cf[0], cf[1], zero4], axis=0)
    gain_in = jnp.concatenate([ci[0], ci[1], zero4], axis=0)
    length = jnp.where(row64 < 2, lens[0], lens[1])
    live = lane64 < length
    forget = jnp.where(live, forget, 0.0)
    span = ck.shape[1]
    tri = jnp.where(iota((span, span), 0) <= iota((span, span), 1), 1.0, 0.0)
    running = dot(forget, tri, precision=lax.Precision.HIGHEST)
    run_last = jnp.sum(forget, axis=1, keepdims=True)
    base = jnp.where(live, run_last - running + gain_in, -jnp.inf)
    base = jnp.where(row64 < 4, base, 0.0)
    base_max = jnp.max(base, axis=1, keepdims=True)
    row1 = iota((8, 1), 0)
    state_top = jnp.where(
        row1 == 0,
        smax[0, 0],
        jnp.where(row1 == 1, smax[0, 1], jnp.where(row1 == 2, smax[1, 0], smax[1, 1])),
    )
    state_base = run_last + state_top
    for i in range(2):
        for h in range(2):
            whole = state[i, h]
            high = whole.astype(BF16)
            split[0, 2 * i + h] = high
            split[1, 2 * i + h] = (whole - high.astype(F32)).astype(BF16)
    size = sn.shape[2]
    zero_rows = jnp.zeros((4, size), F32)
    norm8 = jnp.concatenate([sn[0], sn[1], zero_rows], axis=0)
    halves = [hg[:, :size], hg[:, size:]]
    gain8 = jnp.concatenate(halves + halves + [zero_rows], axis=0)
    pr = iota((4 * seqs, 8 * kvs), 0)
    pc = iota((4 * seqs, 8 * kvs), 1)
    seq, hu = pr % seqs, pr // seqs
    target = (seq // 2) * 8 + (hu % 2) * 4 + (seq % 2) * 2 + hu // 2
    pick[...] = jnp.where(pc == target, 1.0, 0.0).astype(BF16)
    hidden_cols = gw.shape[0]
    gu[...] = jnp.zeros_like(gu)
    gu[:hidden_cols, :] = (gw[...].astype(F32) * mg[...]).astype(BF16)
    gu[HIDDEN_PAD : HIDDEN_PAD + hidden_cols, :] = (uw[...].astype(F32) * mg[...]).astype(BF16)
    group = 128 // width

    def arrange(b, carry):
        block = dw[:, pl.ds(pl.multiple_of(b * 128, 128), 128)].astype(F32)
        block = jnp.concatenate([block, jnp.zeros((HIDDEN_PAD - hidden_cols, 128), F32)], axis=0)
        block = block.T.astype(BF16)
        for k in range(group):
            at_kv = b * group + k
            mirrored = (at_kv % n) * n + at_kv // n
            half = width // 2
            dt[0, at_kv] = block[k * width : k * width + half]
            dt[1, mirrored] = block[k * width + half : (k + 1) * width]
        return carry

    lax.fori_loop(0, kvs // group, arrange, 0)

    own = p1[first].astype(F32)
    for d in order:
        one[d].wait_recv()
    for d in order:
        own = own + r1[d - 1].astype(F32)
    q2f[...] = jnp.zeros_like(q2f)
    for i in range(2):
        part = own[i * n : (i + 1) * n]
        for c in range(KINDS * blocks):
            kind, h, u = c // blocks, (c % blocks) // 2, c % 2
            q2f[pl.ds(kind * 8 + u * 4 + i * 2 + h, n, stride=ROWS), :] = part[
                :, c * 128 : (c + 1) * 128
            ]
        for h in range(2):
            q2f[pl.ds(32 + i * 2 + h, n, stride=ROWS), :] = part[:, KINDS * cols :]
    q2b[...] = q2f[...].reshape(n, ROWS, 128).astype(BF16)
    two = exchange(
        lambda d: q2b.at[lax.rem(second + d, n)], lambda d: r2.at[d - 1], s2, v2, second_peer
    )
    mine = q2f[pl.ds(pl.multiple_of(second * ROWS, 8), ROWS), :]
    for d in order:
        two[d].wait_recv()
    for d in order:
        mine = mine + r2[d - 1].astype(F32)

    def heads(kind):
        a = mine[kind * 8 : kind * 8 + 4]
        b = mine[kind * 8 + 4 : kind * 8 + 8]
        return jnp.concatenate([jnp.concatenate([a, b], axis=1), zero_rows], axis=0)

    gate8 = mine[32:40]
    lane = iota((8, 128), 1)
    row = iota((8, 128), 0)
    square = jnp.sum(jnp.where(lane == 8, gate8, 0.0), axis=1, keepdims=True)
    in_sum = jnp.sum(jnp.where(lane == 2 * tp + row % 2, gate8, 0.0), axis=1, keepdims=True)
    fg_sum = jnp.sum(jnp.where(lane == 4 + 2 * tp + row % 2, gate8, 0.0), axis=1, keepdims=True)
    scale = lax.rsqrt(square / model + EPS)
    query = (scale * heads(0)).astype(BF16).astype(F32)
    key_new = (scale * heads(1)).astype(BF16).astype(F32)
    value_new = (scale * heads(2)).astype(BF16).astype(F32)
    outgate = (scale * heads(3)).astype(BF16).astype(F32)
    in_gate = scale * in_sum
    fg = scale * fg_sum
    forget_new = jnp.minimum(fg, 0.0) - jnp.log1p(jnp.exp(-jnp.abs(fg)))
    weight_log = base + forget_new
    state_log = state_base + forget_new
    peak = jnp.maximum(jnp.maximum(state_log, in_gate), base_max + forget_new)
    query = query * (size**-0.5)
    rows = iota((8, size), 0)
    alone = [jnp.where(rows == k, query, 0.0) for k in range(4)]
    dots = dot(jnp.concatenate(alone[0:2], axis=1).astype(BF16), ck[0], 1, 1)
    dots = dots + dot(jnp.concatenate(alone[2:4], axis=1).astype(BF16), ck[1], 1, 1)
    scores = jnp.exp(weight_log - peak) * dots
    self_score = jnp.exp(in_gate - peak) * jnp.sum(query * key_new, axis=1, keepdims=True)
    carried = jnp.exp(state_log - peak)
    read = dot(alone[0].astype(BF16), split[0, 0], 1, 1)
    read = read + dot(alone[0].astype(BF16), split[1, 0], 1, 1)
    for k in range(1, 4):
        read = read + dot(alone[k].astype(BF16), split[0, k], 1, 1)
        read = read + dot(alone[k].astype(BF16), split[1, k], 1, 1)
    norm_read = jnp.sum(norm8 * query, axis=1, keepdims=True)
    values = dot(jnp.where(row64 < 2, scores, 0.0).astype(BF16), cv[0])
    values = values + dot(jnp.where(row64 >= 2, scores, 0.0).astype(BF16), cv[1])
    values = jnp.where(rows % 2 == 0, values[:, :size], values[:, size:])
    numerator = carried * read + values + self_score * value_new
    denominator = carried * norm_read + jnp.sum(scores, axis=1, keepdims=True) + self_score
    hidden = numerator / jnp.maximum(jnp.abs(denominator), 1.0)
    mixed = hidden * gain8 * jax.nn.sigmoid(outgate)
    mh[kv] = jnp.concatenate([mixed[:4, :128], mixed[:4, 128:]], axis=0).astype(BF16)

    stride = kvs // 2 + 5 if kvs > 8 else 1

    def spread(j, carry):
        peer = lax.rem(kv + lax.rem(j * stride, kvs), kvs)
        pltpu.make_async_remote_copy(
            src_ref=mh.at[kv],
            dst_ref=mh.at[kv],
            send_sem=s3,
            recv_sem=v3,
            device_id=(dp, peer, tp),
            device_id_type=MESH,
        ).start()
        return carry

    lax.fori_loop(1, kvs, spread, 0)
    all_mh = pltpu.make_async_remote_copy(
        src_ref=mh.at[pl.ds(0, kvs - 1)],
        dst_ref=mh.at[pl.ds(0, kvs - 1)],
        send_sem=s3,
        recv_sem=v3,
        device_id=sibling,
        device_id_type=MESH,
    )
    all_mh.wait_recv()

    flat = mh[...].astype(F32).reshape(8 * kvs, 128).astype(BF16)
    picked = dot(pick[...], flat).astype(BF16)
    mix = dot(mixw[:, :128], picked[:seqs], 1, 1)
    for k in range(1, 4):
        mix = mix + dot(mixw[:, k * 128 : (k + 1) * 128], picked[k * seqs : (k + 1) * seqs], 1, 1)
    mix = mix.astype(BF16)
    xs[...] = mix
    swap = pltpu.make_async_remote_copy(
        src_ref=xs,
        dst_ref=xr,
        send_sem=s4,
        recv_sem=v4,
        device_id=sibling,
        device_id_type=MESH,
    )
    swap.start()
    swap.wait_recv()
    total = tok[...].astype(F32) + (mix.astype(F32) + xr[...].astype(F32))
    rbuf[...] = total.astype(BF16).reshape(2, width // 2, seqs)
    rt[kv, tp] = rbuf[tp]

    for dz in order + [0]:

        def send_row(dy, carry, dz=dz):
            peer = lax.rem(z + dz, n) * n + lax.rem(y + dy, n)
            pltpu.make_async_remote_copy(
                src_ref=rbuf.at[tp],
                dst_ref=rt.at[kv, tp],
                send_sem=s5,
                recv_sem=v5.at[dz],
                device_id=(dp, peer, tp),
                device_id_type=MESH,
            ).start()
            return carry

        lax.fori_loop(1 if dz == 0 else 0, n, send_row, 0)

    forward = {}
    for dz in order + [0]:
        count = n - 1 if dz == 0 else n
        pltpu.make_async_remote_copy(
            src_ref=rt.at[pl.ds(0, count), 0],
            dst_ref=rt.at[pl.ds(0, count), 0],
            send_sem=s5,
            recv_sem=v5.at[dz],
            device_id=sibling,
            device_id_type=MESH,
        ).wait_recv()
        source = lax.rem(z + n - dz, n) * n
        forward[dz] = pltpu.make_async_remote_copy(
            src_ref=rt.at[pl.ds(source, n), tp],
            dst_ref=rt.at[pl.ds(source, n), tp],
            send_sem=s6.at[dz],
            recv_sem=v6.at[dz],
            device_id=sibling,
            device_id_type=MESH,
        )
        forward[dz].start()
    for dz in order + [0]:
        forward[dz].wait_recv()

    residual = rt[...].reshape(model, seqs)
    wide = residual.astype(F32)
    power = jnp.sum(wide * wide, axis=0, keepdims=True)
    acc = dot(gu[...], residual)
    scale_mid = lax.rsqrt(power / model + EPS)
    gate = scale_mid * acc[:HIDDEN_PAD]
    up = scale_mid * acc[HIDDEN_PAD:]
    units = (gate * jax.nn.sigmoid(gate) * up).astype(BF16)

    half = width // 2
    other_first = y + (z - y) * tp
    swaps = []
    steps = order + [0]
    for k, d in enumerate(steps):
        at_f = lax.rem(other_first + d, n)
        rows_of = dt[other, pl.ds(at_f * n, n)].reshape(n * half, HIDDEN_PAD)
        xo[k] = dot(rows_of, units).astype(BF16)
        c = pltpu.make_async_remote_copy(
            src_ref=xo.at[k],
            dst_ref=xi.at[k],
            send_sem=s7.at[k],
            recv_sem=v7.at[k],
            device_id=sibling,
            device_id_type=MESH,
        )
        c.start()
        swaps.append(c)
    for k, d in enumerate(steps):
        at_f = lax.rem(first + d, n)
        rows_of = dt[tp, pl.ds(at_f * n, n)].reshape(n * half, HIDDEN_PAD)
        p5[k] = dot(rows_of, units)
    three = {}
    for k, d in enumerate(steps):
        swaps[k].wait_recv()
        both = p5[k] + xi[k].astype(F32)
        if d == 0:
            own = both
            continue
        p5b[k] = both.astype(BF16)
        three[d] = pltpu.make_async_remote_copy(
            src_ref=p5b.at[k],
            dst_ref=r3.at[d - 1],
            send_sem=s8.at[d - 1],
            recv_sem=v8.at[d - 1],
            device_id=first_peer(d),
            device_id_type=MESH,
        )
        three[d].start()
    for d in order:
        three[d].wait_recv()
    for d in order:
        own = own + r3[d - 1].astype(F32)
    own = own.reshape(n, half, seqs)
    p5[0] = own.reshape(n * half, seqs)
    q4b[...] = own.astype(BF16)
    four = exchange(
        lambda d: q4b.at[lax.rem(second + d, n)], lambda d: r4.at[d - 1], s9, v9, second_peer
    )
    last = p5[0, pl.ds(pl.multiple_of(second * half, half), half), :]
    last = last + rt[kv, tp].astype(F32)
    for d in order:
        four[d].wait_recv()
    for d in order:
        last = last + r4[d - 1].astype(F32)
    out_ref[...] = last.astype(BF16)

    for made in (one, two, three, four, forward):
        for c in made.values():
            c.wait_send()
    for c in swaps:
        c.wait_send()
    swap.wait_send()
    all_mh.wait_send()
    pltpu.make_async_remote_copy(
        src_ref=rt.at[pl.ds(0, kvs - 1), 0],
        dst_ref=rt.at[pl.ds(0, kvs - 1), 0],
        send_sem=s5,
        recv_sem=v5.at[0],
        device_id=sibling,
        device_id_type=MESH,
    ).wait_send()


def per_device(n, *args):
    (tokens, pre, qw, kw, vw, ow, ig, fg, ck, cv, ci, cf, lens, sm, sn, smax) = args[:16]
    hg, mixw, mg, gw, uw, dw = args[16:]
    operands = (
        tokens.T,
        pre.reshape(1, -1),
        qw,
        kw,
        vw,
        ow,
        ig.T,
        fg.T,
        ck,
        cv,
        ci.transpose(0, 2, 1),
        cf.transpose(0, 2, 1),
        lens,
        sm,
        sn,
        smax,
        hg.reshape(1, -1),
        mixw.T,
        mg.reshape(1, -1),
        gw.T,
        uw.T,
        dw,
    )
    seqs, width = tokens.shape
    cols = qw.shape[1]
    kvs = n * n
    model = width * kvs
    span, size = ck.shape[1], sn.shape[2]
    wide = KINDS * cols + 128
    half = width // 2
    dma = pltpu.SemaphoreType.DMA
    vmem = pltpu.VMEM
    scratch = [
        vmem((width, seqs), BF16),
        vmem((1, width), F32),
        vmem((KINDS, width, cols), BF16),
        vmem((2, 4, model), BF16),
        vmem((2, span, cols), BF16),
        vmem((2, span, cols), BF16),
        vmem((2, 2, span), F32),
        vmem((2, 2, span), F32),
        pltpu.SMEM((2,), jnp.int32),
        vmem((2, 2, size, size), F32),
        vmem((2, 2, size), F32),
        pltpu.SMEM((2, 2), F32),
        vmem((1, cols), F32),
        vmem((width, cols), BF16),
        vmem((1, model), F32),
        vmem((gw.shape[1], model), BF16),
        vmem((gw.shape[1], model), BF16),
        vmem((gw.shape[1], model), BF16),
        dma((22,)),
        vmem((n, 2 * n, wide), BF16),
        vmem((n - 1, 2 * n, wide), BF16),
        vmem((n * ROWS, 128), F32),
        vmem((n, ROWS, 128), BF16),
        vmem((n - 1, ROWS, 128), BF16),
        vmem((2, 4, size, size), BF16),
        vmem((4 * seqs, 8 * kvs), BF16),
        vmem((kvs, 8, 128), BF16),
        vmem((width, seqs), BF16),
        vmem((width, seqs), BF16),
        vmem((2, half, seqs), BF16),
        vmem((kvs, 2, half, seqs), BF16),
        vmem((2 * HIDDEN_PAD, model), BF16),
        vmem((2, kvs, half, HIDDEN_PAD), BF16),
        vmem((n, n * half, seqs), BF16),
        vmem((n, n * half, seqs), BF16),
        vmem((n, n * half, seqs), F32),
        vmem((n, n * half, seqs), BF16),
        vmem((n - 1, n * half, seqs), BF16),
        vmem((n, half, seqs), BF16),
        vmem((n - 1, half, seqs), BF16),
        dma((n - 1,)),
        dma((n - 1,)),
        dma((n - 1,)),
        dma((n - 1,)),
        dma,
        dma,
        dma,
        dma,
        dma,
        dma((n,)),
        dma((n,)),
        dma((n,)),
        dma((n,)),
        dma((n,)),
        dma((n - 1,)),
        dma((n - 1,)),
        dma((n - 1,)),
        dma((n - 1,)),
    ]
    out = pl.pallas_call(
        functools.partial(kernel, n),
        out_shape=jax.ShapeDtypeStruct((half, seqs), BF16),
        in_specs=[pl.BlockSpec(memory_space=pl.ANY)] * len(operands),
        out_specs=pl.BlockSpec(memory_space=pltpu.VMEM),
        scratch_shapes=scratch,
        compiler_params=pltpu.CompilerParams(
            collective_id=0, has_side_effects=True, vmem_limit_bytes=62 * 1024 * 1024
        ),
        name="layer",
    )(*operands)
    return out.T


def solution(mesh):
    n = round(mesh.shape["kv"] ** 0.5)
    seq = ("dp", "kv")
    return jax.shard_map(
        functools.partial(per_device, n),
        mesh=mesh,
        in_specs=(
            P("dp", "kv"),
            P("kv"),
            P("kv", "tp"),
            P("kv", "tp"),
            P("kv", "tp"),
            P("kv", "tp"),
            P(),
            P(),
            P(seq, None, "tp"),
            P(seq, None, "tp"),
            P(seq, None, "tp"),
            P(seq, None, "tp"),
            P(seq),
            P(seq, "tp", None, None),
            P(seq, "tp", None),
            P(seq, "tp"),
            P("tp"),
            P("tp", "kv"),
            P(),
            P(None, ("kv", "tp")),
            P(None, ("kv", "tp")),
            P(("kv", "tp"), None),
        ),
        out_specs=P("dp", ("kv", "tp")),
        check_vma=False,
    )
```

time: 125 us -> 62.8 us (0.50)
  Pallas kernels: 0 us -> 60.9 us
  waiting for transfers between devices: 39.5 us -> 0 us
  blocking collectives: 33.8 us -> 0 us
  starting transfers between devices: 29 us -> 0 us
  local copies, waits for them, and re-layouts: 10.9 us -> 1.28 us
  matrix products: 5.88 us -> 0 us
  other arithmetic: 3.99 us -> 0 us
    pallas_call x0 -> x1, Pallas kernels: none -> 60.9 us  [per_device(): pl.pallas_call(functools.partial(kernel, n), out_shape=jax.ShapeDtypeStru...]
    all_to_all x3 -> x0, waiting for transfers between devices: 39.5 us -> none  [the longest x2 22.3 us: from_everyone(): return lax.all_to_all(copies, axis, split_axis=0, concat_axis=0, tiled=True)]
    all_to_all x4 -> x0, blocking collectives: 33.8 us -> none  [the longest x3 27.6 us: sum_at_owner(): lax.all_to_all(in_blocks(shard, dim, length), axis, 0, 0, tiled=True)]
    all_to_all x3 -> x0, starting transfers between devices: 29 us -> none  [the longest x1 17.3 us: sum_at_owner(): lax.all_to_all(in_blocks(shard, dim, length), axis, 0, 0, tiled=True)]
    dot_general x13 -> x0, matrix products: 5.88 us -> none  [the longest x5 3.6 us: product(): return jnp.dot(normed, weight, preferred_element_type=jnp.float32)]
    dynamic_slice x5 -> x0, local copies, waits for them, and re-layouts: 3.77 us -> none  [the longest x3 2.18 us: per_device(): lax.dynamic_slice_in_dim(down_grid, which_half * block_width, block_width...]
    concatenate x5 -> x0, local copies, waits for them, and re-layouts: 3.28 us -> none  [in_one_piece(): jnp.concatenate([a.reshape(*a.shape[:along], w) for a, w in zip(arrays, w...]
    reduce_sum x7 -> x0, other arithmetic: 1.82 us -> none  [the longest x1 0.72 us: per_device(): squares = jnp.sum(token_values * token_values, axis=1)]
  transfers between devices with their start and end apart: 3 -> 0, of which waited for: 3 -> 0; matrix products, arithmetic and copies ran while one was open for 2% -> 0% of each run, Pallas kernels for 0% -> 0%
where the time goes in v1:
time: 62.8 us; the launch traced here: 62.1 us
  Pallas kernels  60.9 us (97%)
  local copies, waits for them, and re-layouts  1.28 us (2%)
    pallas_call x1, Pallas kernels, per_device(): pl.pallas_call(functools.partial(kernel, n), out_shape=jax.ShapeDtypeStru...  60.9 us
    unnamed x1, local copies, waits for them, and re-layouts  1.28 us

profile of v1, /device:TPU:1, one launch (start us, length us, event | category | flops | bytes accessed | tf_op | source)
XLA Modules:
  0.0 62.1 jit_solution(7813588795490358986)
XLA Ops:
  0.0 60.9 %layer.1 = bf16[16,128]{1,0:T(8,128)(2,1)} custom-call(bf16[32,128]{1,0:T(8,128)(2,1)} %bitcast.18, f32[1,32]{1,0:T(1,128)} %bitcast.23, bf16[32,512]{1,0:T(8,128)(2,1)} %qw_h.1, bf16[32,512]{1,0:T(8,128)(2,1)} %kw_h.1, bf16[32,512]{1,0:T(8,128)(2,1)} %vw_h.1, bf16[32,512]{1,0:T(8,128)(2,1)} %ow_h.1, bf16[4,2048]{1,0:T(4,128)(2,1)} %bitcast.15, ...), custom_call_target="tpu_custom_call" | custom-call | tf_op jit(solution)/shard_map/layer/pallas_call | solution.py:615
  60.9 1.3 %copy.24 = bf16[128,16]{0,1:T(8,128)(2,1)} copy(bf16[128,16]{0,1:T(8,128)(2,1)} %bitcast.17) | data formatting | bytes 8192

commit v2 on v1

--- a/solution.py
+++ b/solution.py
@@ -14,10 +14,19 @@
 KINDS = 4
 ROWS = 40
 HIDDEN_PAD = 48
+LAG = 3
 
 
 def ring_order(n):
     return sorted(range(1, n), key=lambda d: (-min(d, n - d), d))
+
+
+def plane_order(n):
+    def hops(d):
+        return min(d, n - d)
+
+    pairs = [(dz, dy) for dz in range(n) for dy in range(n) if dz or dy]
+    return sorted(pairs, key=lambda p: (-hops(p[0]) - hops(p[1]), (3 * p[0] + 5 * p[1]) % n))
 
 
 def dot(a, b, ca=1, cb=0, precision=None):
@@ -84,6 +93,8 @@
     mh,
     xs,
     xr,
+    wg,
+    tg,
     rbuf,
     rt,
     gu,
@@ -113,6 +124,10 @@
     v8,
     s9,
     v9,
+    sw,
+    vw,
+    st,
+    vt,
 ):
     kvs = n * n
     width = tok.shape[0]
@@ -295,6 +310,46 @@
     q2b[...] = q2f[...].reshape(n, ROWS, 128).astype(BF16)
     two = exchange(
         lambda d: q2b.at[lax.rem(second + d, n)], lambda d: r2.at[d - 1], s2, v2, second_peer
+    )
+    half = width // 2
+    axes = ((0, y, lambda d: z * n + lax.rem(y + d, n)), (1, z, lambda d: lax.rem(z + d, n) * n + y))
+    for u, place, peer in axes:
+        for d in order:
+            pltpu.make_async_remote_copy(
+                src_ref=mixw.at[pl.ds(u * half, half)],
+                dst_ref=wg.at[u, place],
+                send_sem=sw,
+                recv_sem=vw,
+                device_id=(dp, peer(d), tp),
+                device_id_type=MESH,
+            ).start()
+        wg[u, place] = mixw[u * half : (u + 1) * half, :]
+    own_rows = pl.ds(pl.multiple_of(tp * half, half), half)
+    for d in order:
+        pltpu.make_async_remote_copy(
+            src_ref=tok.at[own_rows],
+            dst_ref=tg.at[second],
+            send_sem=st,
+            recv_sem=vt,
+            device_id=second_peer(d),
+            device_id_type=MESH,
+        ).start()
+    tg[second] = tok[own_rows, :]
+    all_wg = pltpu.make_async_remote_copy(
+        src_ref=wg.at[:, pl.ds(0, n - 1)],
+        dst_ref=wg.at[:, pl.ds(0, n - 1)],
+        send_sem=sw,
+        recv_sem=vw,
+        device_id=sibling,
+        device_id_type=MESH,
+    )
+    all_tg = pltpu.make_async_remote_copy(
+        src_ref=tg.at[pl.ds(0, n - 1)],
+        dst_ref=tg.at[pl.ds(0, n - 1)],
+        send_sem=st,
+        recv_sem=vt,
+        device_id=sibling,
+        device_id_type=MESH,
     )
     mine = q2f[pl.ds(pl.multiple_of(second * ROWS, 8), ROWS), :]
     for d in order:
@@ -347,21 +402,15 @@
     mixed = hidden * gain8 * jax.nn.sigmoid(outgate)
     mh[kv] = jnp.concatenate([mixed[:4, :128], mixed[:4, 128:]], axis=0).astype(BF16)
 
-    stride = kvs // 2 + 5 if kvs > 8 else 1
-
-    def spread(j, carry):
-        peer = lax.rem(kv + lax.rem(j * stride, kvs), kvs)
+    for dz, dy in plane_order(n):
         pltpu.make_async_remote_copy(
             src_ref=mh.at[kv],
             dst_ref=mh.at[kv],
             send_sem=s3,
             recv_sem=v3,
-            device_id=(dp, peer, tp),
+            device_id=(dp, lax.rem(z + dz, n) * n + lax.rem(y + dy, n), tp),
             device_id_type=MESH,
         ).start()
-        return carry
-
-    lax.fori_loop(1, kvs, spread, 0)
     all_mh = pltpu.make_async_remote_copy(
         src_ref=mh.at[pl.ds(0, kvs - 1)],
         dst_ref=mh.at[pl.ds(0, kvs - 1)],
@@ -370,15 +419,22 @@
         device_id=sibling,
         device_id_type=MESH,
     )
+    all_wg.wait_recv()
+    all_tg.wait_recv()
     all_mh.wait_recv()
 
     flat = mh[...].astype(F32).reshape(8 * kvs, 128).astype(BF16)
     picked = dot(pick[...], flat).astype(BF16)
-    mix = dot(mixw[:, :128], picked[:seqs], 1, 1)
-    for k in range(1, 4):
-        mix = mix + dot(mixw[:, k * 128 : (k + 1) * 128], picked[k * seqs : (k + 1) * seqs], 1, 1)
-    mix = mix.astype(BF16)
-    xs[...] = mix
+
+    def project(u):
+        w = wg[u].reshape(n * half, cols)
+        total = dot(w[:, :128], picked[:seqs], 1, 1)
+        for k in range(1, 4):
+            block = picked[k * seqs : (k + 1) * seqs]
+            total = total + dot(w[:, k * 128 : (k + 1) * 128], block, 1, 1)
+        return total.astype(BF16)
+
+    xs[...] = project(other)
     swap = pltpu.make_async_remote_copy(
         src_ref=xs,
         dst_ref=xr,
@@ -388,50 +444,53 @@
         device_id_type=MESH,
     )
     swap.start()
+    mix = project(tp)
     swap.wait_recv()
-    total = tok[...].astype(F32) + (mix.astype(F32) + xr[...].astype(F32))
-    rbuf[...] = total.astype(BF16).reshape(2, width // 2, seqs)
-    rt[kv, tp] = rbuf[tp]
-
-    for dz in order + [0]:
-
-        def send_row(dy, carry, dz=dz):
-            peer = lax.rem(z + dz, n) * n + lax.rem(y + dy, n)
+    total = tg[...].reshape(n * half, seqs).astype(F32) + (mix.astype(F32) + xr[...].astype(F32))
+    rbuf[...] = total.astype(BF16).reshape(n, half, seqs)
+
+    def gather(u):
+        def rows(f):
+            return rt.at[f, :, 0] if u == 0 else rt.at[:, f, 1]
+
+        made = exchange(lambda d: rbuf, lambda d: rows(first), s5, v5, first_peer)
+        if u == 0:
+            rt[z, :, 0] = rbuf[...]
+        else:
+            rt[:, y, 1] = rbuf[...]
+        for d in [0] + order[::-1]:
+            if d:
+                made[d].wait_recv()
+            source = lax.rem(first + n - d, n)
             pltpu.make_async_remote_copy(
-                src_ref=rbuf.at[tp],
-                dst_ref=rt.at[kv, tp],
-                send_sem=s5,
-                recv_sem=v5.at[dz],
-                device_id=(dp, peer, tp),
+                src_ref=rows(source),
+                dst_ref=rows(source),
+                send_sem=s6.at[d],
+                recv_sem=v6.at[d],
+                device_id=sibling,
                 device_id_type=MESH,
             ).start()
-            return carry
-
-        lax.fori_loop(1 if dz == 0 else 0, n, send_row, 0)
-
-    forward = {}
-    for dz in order + [0]:
-        count = n - 1 if dz == 0 else n
-        pltpu.make_async_remote_copy(
-            src_ref=rt.at[pl.ds(0, count), 0],
-            dst_ref=rt.at[pl.ds(0, count), 0],
-            send_sem=s5,
-            recv_sem=v5.at[dz],
-            device_id=sibling,
-            device_id_type=MESH,
-        ).wait_recv()
-        source = lax.rem(z + n - dz, n) * n
-        forward[dz] = pltpu.make_async_remote_copy(
-            src_ref=rt.at[pl.ds(source, n), tp],
-            dst_ref=rt.at[pl.ds(source, n), tp],
-            send_sem=s6.at[dz],
-            recv_sem=v6.at[dz],
+
+    @pl.when(tp == 0)
+    def _():
+        gather(0)
+
+    @pl.when(tp == 1)
+    def _():
+        gather(1)
+
+    def block_copy(send, recv):
+        return pltpu.make_async_remote_copy(
+            src_ref=rbuf,
+            dst_ref=rt.at[0, :, 0],
+            send_sem=send,
+            recv_sem=recv,
             device_id=sibling,
             device_id_type=MESH,
         )
-        forward[dz].start()
-    for dz in order + [0]:
-        forward[dz].wait_recv()
+
+    for d in range(n):
+        block_copy(s6.at[d], v6.at[d]).wait_recv()
 
     residual = rt[...].reshape(model, seqs)
     wide = residual.astype(F32)
@@ -442,10 +501,29 @@
     up = scale_mid * acc[HIDDEN_PAD:]
     units = (gate * jax.nn.sigmoid(gate) * up).astype(BF16)
 
-    half = width // 2
     other_first = y + (z - y) * tp
     swaps = []
     steps = order + [0]
+    three = {}
+
+    def finish(k):
+        swaps[k].wait_recv()
+        both = p5[k] + xi[k].astype(F32)
+        d = steps[k]
+        if d == 0:
+            return both
+        p5b[k] = both.astype(BF16)
+        three[d] = pltpu.make_async_remote_copy(
+            src_ref=p5b.at[k],
+            dst_ref=r3.at[d - 1],
+            send_sem=s8.at[d - 1],
+            recv_sem=v8.at[d - 1],
+            device_id=first_peer(d),
+            device_id_type=MESH,
+        )
+        three[d].start()
+        return None
+
     for k, d in enumerate(steps):
         at_f = lax.rem(other_first + d, n)
         rows_of = dt[other, pl.ds(at_f * n, n)].reshape(n * half, HIDDEN_PAD)
@@ -460,27 +538,13 @@
         )
         c.start()
         swaps.append(c)
-    for k, d in enumerate(steps):
         at_f = lax.rem(first + d, n)
         rows_of = dt[tp, pl.ds(at_f * n, n)].reshape(n * half, HIDDEN_PAD)
         p5[k] = dot(rows_of, units)
-    three = {}
-    for k, d in enumerate(steps):
-        swaps[k].wait_recv()
-        both = p5[k] + xi[k].astype(F32)
-        if d == 0:
-            own = both
-            continue
-        p5b[k] = both.astype(BF16)
-        three[d] = pltpu.make_async_remote_copy(
-            src_ref=p5b.at[k],
-            dst_ref=r3.at[d - 1],
-            send_sem=s8.at[d - 1],
-            recv_sem=v8.at[d - 1],
-            device_id=first_peer(d),
-            device_id_type=MESH,
-        )
-        three[d].start()
+        if k >= LAG:
+            finish(k - LAG)
+    for k in range(max(0, n - LAG), n):
+        own = finish(k)
     for d in order:
         three[d].wait_recv()
     for d in order:
@@ -492,28 +556,24 @@
         lambda d: q4b.at[lax.rem(second + d, n)], lambda d: r4.at[d - 1], s9, v9, second_peer
     )
     last = p5[0, pl.ds(pl.multiple_of(second * half, half), half), :]
-    last = last + rt[kv, tp].astype(F32)
+    last = last + rt[z, y, tp].astype(F32)
     for d in order:
         four[d].wait_recv()
     for d in order:
         last = last + r4[d - 1].astype(F32)
     out_ref[...] = last.astype(BF16)
 
-    for made in (one, two, three, four, forward):
+    for made in (one, two, three, four):
         for c in made.values():
             c.wait_send()
     for c in swaps:
         c.wait_send()
-    swap.wait_send()
-    all_mh.wait_send()
-    pltpu.make_async_remote_copy(
-        src_ref=rt.at[pl.ds(0, kvs - 1), 0],
-        dst_ref=rt.at[pl.ds(0, kvs - 1), 0],
-        send_sem=s5,
-        recv_sem=v5.at[0],
-        device_id=sibling,
-        device_id_type=MESH,
-    ).wait_send()
+    for c in (swap, all_mh, all_wg, all_tg):
+        c.wait_send()
+    for d in range(1, n):
+        block_copy(s5.at[d - 1], v5.at[d - 1]).wait_send()
+    for d in range(n):
+        block_copy(s6.at[d], v6.at[d]).wait_send()
 
 
 def per_device(n, *args):
@@ -580,10 +640,12 @@
         vmem((2, 4, size, size), BF16),
         vmem((4 * seqs, 8 * kvs), BF16),
         vmem((kvs, 8, 128), BF16),
-        vmem((width, seqs), BF16),
-        vmem((width, seqs), BF16),
-        vmem((2, half, seqs), BF16),
-        vmem((kvs, 2, half, seqs), BF16),
+        vmem((n * half, seqs), BF16),
+        vmem((n * half, seqs), BF16),
+        vmem((2, n, half, cols), BF16),
+        vmem((n, half, seqs), BF16),
+        vmem((n, half, seqs), BF16),
+        vmem((n, n, 2, half, seqs), BF16),
         vmem((2 * HIDDEN_PAD, model), BF16),
         vmem((2, kvs, half, HIDDEN_PAD), BF16),
         vmem((n, n * half, seqs), BF16),
@@ -601,16 +663,20 @@
         dma,
         dma,
         dma,
-        dma,
+        dma((n - 1,)),
+        dma((n - 1,)),
         dma((n,)),
         dma((n,)),
         dma((n,)),
         dma((n,)),
-        dma((n,)),
-        dma((n - 1,)),
-        dma((n - 1,)),
-        dma((n - 1,)),
-        dma((n - 1,)),
+        dma((n - 1,)),
+        dma((n - 1,)),
+        dma((n - 1,)),
+        dma((n - 1,)),
+        dma,
+        dma,
+        dma,
+        dma,
     ]
     out = pl.pallas_call(
         functools.partial(kernel, n),

time: 62.8 us -> 59.1 us (0.941)
  Pallas kernels: 60.9 us -> 57.5 us
    pallas_call x1, Pallas kernels: 60.9 us -> 57.5 us  [per_device(): pl.pallas_call(functools.partial(kernel, n), out_shape=jax.ShapeDtypeStru...]
where the time goes in v2:
time: 59.1 us; the launch traced here: 58.8 us
  Pallas kernels  57.5 us (97%)
  local copies, waits for them, and re-layouts  1.28 us (2%)
    pallas_call x1, Pallas kernels, per_device(): pl.pallas_call(functools.partial(kernel, n), out_shape=jax.ShapeDtypeStru...  57.5 us
    unnamed x1, local copies, waits for them, and re-layouts  1.28 us

profile of v2, /device:TPU:1, one launch (start us, length us, event | category | flops | bytes accessed | tf_op | source)
XLA Modules:
  0.0 58.8 jit_solution(2762691007075584637)
XLA Ops:
  0.0 57.5 %layer.1 = bf16[16,128]{1,0:T(8,128)(2,1)} custom-call(bf16[32,128]{1,0:T(8,128)(2,1)} %bitcast.18, f32[1,32]{1,0:T(1,128)} %bitcast.23, bf16[32,512]{1,0:T(8,128)(2,1)} %qw_h.1, bf16[32,512]{1,0:T(8,128)(2,1)} %kw_h.1, bf16[32,512]{1,0:T(8,128)(2,1)} %vw_h.1, bf16[32,512]{1,0:T(8,128)(2,1)} %ow_h.1, bf16[4,2048]{1,0:T(4,128)(2,1)} %bitcast.15, ...), custom_call_target="tpu_custom_call" | custom-call | tf_op jit(solution)/shard_map/layer/pallas_call | solution.py:681
  57.5 1.3 %copy.24 = bf16[128,16]{0,1:T(8,128)(2,1)} copy(bf16[128,16]{0,1:T(8,128)(2,1)} %bitcast.17) | data formatting | bytes 8192

commit v3 on v2

--- a/solution.py
+++ b/solution.py
@@ -14,7 +14,6 @@
 KINDS = 4
 ROWS = 40
 HIDDEN_PAD = 48
-LAG = 3
 
 
 def ring_order(n):
@@ -85,6 +84,8 @@
     load_sem,
     p1,
     r1,
+    relay,
+    merged,
     q2f,
     q2b,
     r2,
@@ -104,8 +105,7 @@
     p5,
     p5b,
     r3,
-    q4b,
-    r4,
+    result,
     s1,
     v1,
     s2,
@@ -123,16 +123,20 @@
     s8,
     v8,
     s9,
-    v9,
     sw,
     vw,
     st,
     vt,
+    sr,
+    vr,
+    s10,
+    v10,
 ):
     kvs = n * n
     width = tok.shape[0]
     seqs = tok.shape[1]
     cols = w4.shape[2]
+    wide = p1.shape[2]
     blocks = cols // 128
     model = width * kvs
     dp = lax.axis_index("dp")
@@ -153,12 +157,6 @@
         return (dp, first * far + lax.rem(second + d, n) * near, tp)
 
     sibling = (dp, kv, other)
-
-    barrier = pltpu.get_barrier_semaphore()
-    for d in range(1, n):
-        pl.semaphore_signal(barrier, inc=1, device_id=first_peer(d), device_id_type=MESH)
-        pl.semaphore_signal(barrier, inc=1, device_id=second_peer(d), device_id_type=MESH)
-    pl.semaphore_signal(barrier, inc=1, device_id=sibling, device_id_type=MESH)
 
     loads = [
         (tok_h, tok),
@@ -185,7 +183,14 @@
         (dw_h, dw),
     ]
     copies = [pltpu.make_async_copy(a, b, load_sem.at[k]) for k, (a, b) in enumerate(loads)]
-    for c in copies:
+    for c in copies[:8]:
+        c.start()
+    barrier = pltpu.get_barrier_semaphore()
+    for d in range(1, n):
+        pl.semaphore_signal(barrier, inc=1, device_id=first_peer(d), device_id_type=MESH)
+        pl.semaphore_signal(barrier, inc=1, device_id=second_peer(d), device_id_type=MESH)
+    pl.semaphore_signal(barrier, inc=1, device_id=sibling, device_id_type=MESH)
+    for c in copies[8:]:
         c.start()
     for c in copies[:8]:
         c.wait()
@@ -228,9 +233,51 @@
             made[d].start()
         return made
 
-    one = exchange(
-        lambda d: p1.at[lax.rem(first + d, n)], lambda d: r1.at[d - 1], s1, v1, first_peer
-    )
+    far_d = n // 2
+    cut = (KINDS * blocks // 2 + 1) * 128
+    parts = (pl.ds(0, cut), pl.ds(cut, wide - cut))
+
+    def part_copy(src, dst, peer, send, recv, k):
+        return pltpu.make_async_remote_copy(
+            src_ref=src.at[:, parts[k]],
+            dst_ref=dst.at[:, parts[k]],
+            send_sem=send,
+            recv_sem=recv,
+            device_id=first_peer(peer),
+            device_id_type=MESH,
+        )
+
+    def rows_for(d):
+        return p1.at[lax.rem(first + d, n)]
+
+    hops = (n - 1, 1)
+    last_d = (far_d + 1, far_d - 1)
+    handed = [
+        part_copy(rows_for(far_d), relay, hops[k], sr.at[k], vr.at[k], k) for k in range(2)
+    ]
+    for c in handed:
+        c.start()
+    one = []
+    for k in range(2):
+        d = last_d[k]
+        one.append(
+            part_copy(rows_for(d), r1.at[d - 1], d, s1.at[d - 1], v1.at[d - 1], 1 - k)
+        )
+    for d in order:
+        if d == far_d or d in last_d:
+            continue
+        one.append(
+            pltpu.make_async_remote_copy(
+                src_ref=rows_for(d),
+                dst_ref=r1.at[d - 1],
+                send_sem=s1.at[d - 1],
+                recv_sem=v1.at[d - 1],
+                device_id=first_peer(d),
+                device_id_type=MESH,
+            )
+        )
+    for c in one[:-2]:
+        c.start()
 
     for c in copies[8:]:
         c.wait()
@@ -292,11 +339,25 @@
 
     lax.fori_loop(0, kvs // group, arrange, 0)
 
+    late = []
+    late_sems = ((s1.at[far_d - 1], v1.at[far_d - 1]), (s10, v10))
+    for k in range(2):
+        d = last_d[k]
+        handed[k].wait_recv()
+        mine = p1[lax.rem(first + d, n), :, parts[k]].astype(F32)
+        merged[:, parts[k]] = (mine + relay[:, parts[k]].astype(F32)).astype(BF16)
+        c = part_copy(merged, r1.at[d - 1], d, late_sems[k][0], late_sems[k][1], k)
+        c.start()
+        late.append(c)
+    for c in one[-2:]:
+        c.start()
+    one = one + late
     own = p1[first].astype(F32)
+    for c in one:
+        c.wait_recv()
     for d in order:
-        one[d].wait_recv()
-    for d in order:
-        own = own + r1[d - 1].astype(F32)
+        if d != far_d:
+            own = own + r1[d - 1].astype(F32)
     q2f[...] = jnp.zeros_like(q2f)
     for i in range(2):
         part = own[i * n : (i + 1) * n]
@@ -493,8 +554,8 @@
         block_copy(s6.at[d], v6.at[d]).wait_recv()
 
     residual = rt[...].reshape(model, seqs)
-    wide = residual.astype(F32)
-    power = jnp.sum(wide * wide, axis=0, keepdims=True)
+    spread = residual.astype(F32)
+    power = jnp.sum(spread * spread, axis=0, keepdims=True)
     acc = dot(gu[...], residual)
     scale_mid = lax.rsqrt(power / model + EPS)
     gate = scale_mid * acc[:HIDDEN_PAD]
@@ -502,34 +563,13 @@
     units = (gate * jax.nn.sigmoid(gate) * up).astype(BF16)
 
     other_first = y + (z - y) * tp
+    steps = order + [0]
+    whole = dot(dt[other].reshape(kvs * half, HIDDEN_PAD), units)
+    xo[...] = whole.astype(BF16).reshape(n, n * half, seqs)
     swaps = []
-    steps = order + [0]
-    three = {}
-
-    def finish(k):
-        swaps[k].wait_recv()
-        both = p5[k] + xi[k].astype(F32)
-        d = steps[k]
-        if d == 0:
-            return both
-        p5b[k] = both.astype(BF16)
-        three[d] = pltpu.make_async_remote_copy(
-            src_ref=p5b.at[k],
-            dst_ref=r3.at[d - 1],
-            send_sem=s8.at[d - 1],
-            recv_sem=v8.at[d - 1],
-            device_id=first_peer(d),
-            device_id_type=MESH,
-        )
-        three[d].start()
-        return None
-
     for k, d in enumerate(steps):
-        at_f = lax.rem(other_first + d, n)
-        rows_of = dt[other, pl.ds(at_f * n, n)].reshape(n * half, HIDDEN_PAD)
-        xo[k] = dot(rows_of, units).astype(BF16)
         c = pltpu.make_async_remote_copy(
-            src_ref=xo.at[k],
+            src_ref=xo.at[lax.rem(other_first + d, n)],
             dst_ref=xi.at[k],
             send_sem=s7.at[k],
             recv_sem=v7.at[k],
@@ -538,42 +578,54 @@
         )
         c.start()
         swaps.append(c)
+    p5[...] = dot(dt[tp].reshape(kvs * half, HIDDEN_PAD), units).reshape(n, n * half, seqs)
+    for k, d in enumerate(steps):
+        swaps[k].wait_recv()
         at_f = lax.rem(first + d, n)
-        rows_of = dt[tp, pl.ds(at_f * n, n)].reshape(n * half, HIDDEN_PAD)
-        p5[k] = dot(rows_of, units)
-        if k >= LAG:
-            finish(k - LAG)
-    for k in range(max(0, n - LAG), n):
-        own = finish(k)
-    for d in order:
-        three[d].wait_recv()
-    for d in order:
-        own = own + r3[d - 1].astype(F32)
-    own = own.reshape(n, half, seqs)
-    p5[0] = own.reshape(n * half, seqs)
-    q4b[...] = own.astype(BF16)
-    four = exchange(
-        lambda d: q4b.at[lax.rem(second + d, n)], lambda d: r4.at[d - 1], s9, v9, second_peer
-    )
-    last = p5[0, pl.ds(pl.multiple_of(second * half, half), half), :]
+        both = p5[at_f] + xi[k].astype(F32)
+        p5b[k] = both.astype(BF16).reshape(n, half, seqs)
+        if d == 0:
+            p5[at_f] = both
+        for e in steps:
+            if d or e:
+                at_s = lax.rem(second + e, n)
+                pltpu.make_async_remote_copy(
+                    src_ref=p5b.at[k, at_s],
+                    dst_ref=r3.at[d * n + e - 1],
+                    send_sem=s8,
+                    recv_sem=v8,
+                    device_id=(dp, at_f * far + at_s * near, tp),
+                    device_id_type=MESH,
+                ).start()
+    last = p5[first, pl.ds(pl.multiple_of(second * half, half), half), :]
     last = last + rt[z, y, tp].astype(F32)
-    for d in order:
-        four[d].wait_recv()
-    for d in order:
-        last = last + r4[d - 1].astype(F32)
-    out_ref[...] = last.astype(BF16)
-
-    for made in (one, two, three, four):
-        for c in made.values():
-            c.wait_send()
+    all_r3 = pltpu.make_async_remote_copy(
+        src_ref=r3,
+        dst_ref=r3,
+        send_sem=s8,
+        recv_sem=v8,
+        device_id=sibling,
+        device_id_type=MESH,
+    )
+    all_r3.wait_recv()
+    last = last + jnp.sum(r3[...].astype(F32), axis=0)
+    result[...] = last.astype(BF16)
+    written = pltpu.make_async_copy(result, out_ref, s9)
+    written.start()
+
+    for c in two.values():
+        c.wait_send()
+    for c in one + handed:
+        c.wait_send()
     for c in swaps:
         c.wait_send()
-    for c in (swap, all_mh, all_wg, all_tg):
+    for c in (swap, all_mh, all_wg, all_tg, all_r3):
         c.wait_send()
     for d in range(1, n):
         block_copy(s5.at[d - 1], v5.at[d - 1]).wait_send()
     for d in range(n):
         block_copy(s6.at[d], v6.at[d]).wait_send()
+    written.wait()
 
 
 def per_device(n, *args):
@@ -634,6 +686,8 @@
         dma((22,)),
         vmem((n, 2 * n, wide), BF16),
         vmem((n - 1, 2 * n, wide), BF16),
+        vmem((2 * n, wide), BF16),
+        vmem((2 * n, wide), BF16),
         vmem((n * ROWS, 128), F32),
         vmem((n, ROWS, 128), BF16),
         vmem((n - 1, ROWS, 128), BF16),
@@ -651,10 +705,9 @@
         vmem((n, n * half, seqs), BF16),
         vmem((n, n * half, seqs), BF16),
         vmem((n, n * half, seqs), F32),
-        vmem((n, n * half, seqs), BF16),
-        vmem((n - 1, n * half, seqs), BF16),
-        vmem((n, half, seqs), BF16),
-        vmem((n - 1, half, seqs), BF16),
+        vmem((n, n, half, seqs), BF16),
+        vmem((kvs - 1, half, seqs), BF16),
+        vmem((half, seqs), BF16),
         dma((n - 1,)),
         dma((n - 1,)),
         dma((n - 1,)),
@@ -669,12 +722,15 @@
         dma((n,)),
         dma((n,)),
         dma((n,)),
-        dma((n - 1,)),
-        dma((n - 1,)),
-        dma((n - 1,)),
-        dma((n - 1,)),
-        dma,
-        dma,
+        dma,
+        dma,
+        dma,
+        dma,
+        dma,
+        dma,
+        dma,
+        dma((2,)),
+        dma((2,)),
         dma,
         dma,
     ]
@@ -682,7 +738,7 @@
         functools.partial(kernel, n),
         out_shape=jax.ShapeDtypeStruct((half, seqs), BF16),
         in_specs=[pl.BlockSpec(memory_space=pl.ANY)] * len(operands),
-        out_specs=pl.BlockSpec(memory_space=pltpu.VMEM),
+        out_specs=pl.BlockSpec(memory_space=pl.ANY),
         scratch_shapes=scratch,
         compiler_params=pltpu.CompilerParams(
             collective_id=0, has_side_effects=True, vmem_limit_bytes=62 * 1024 * 1024

time: 59.1 us -> 57.7 us (0.976)
  Pallas kernels: 57.5 us -> 56.2 us
    pallas_call x1, Pallas kernels: 57.5 us -> 56.2 us  [per_device(): pl.pallas_call(functools.partial(kernel, n), out_shape=jax.ShapeDtypeStru...]
where the time goes in v3:
time: 57.7 us; the launch traced here: 57.5 us
  Pallas kernels  56.2 us (97%)
  local copies, waits for them, and re-layouts  1.28 us (2%)
    pallas_call x1, Pallas kernels, per_device(): pl.pallas_call(functools.partial(kernel, n), out_shape=jax.ShapeDtypeStru...  56.2 us
    unnamed x1, local copies, waits for them, and re-layouts  1.28 us

profile of v3, /device:TPU:1, one launch (start us, length us, event | category | flops | bytes accessed | tf_op | source)
XLA Modules:
  0.0 57.5 jit_solution(1709205870589336977)
XLA Ops:
  0.0 56.2 %layer.1 = bf16[16,128]{1,0:T(8,128)(2,1)} custom-call(bf16[32,128]{1,0:T(8,128)(2,1)} %bitcast.18, f32[1,32]{1,0:T(1,128)} %bitcast.23, bf16[32,512]{1,0:T(8,128)(2,1)} %qw_h.1, bf16[32,512]{1,0:T(8,128)(2,1)} %kw_h.1, bf16[32,512]{1,0:T(8,128)(2,1)} %vw_h.1, bf16[32,512]{1,0:T(8,128)(2,1)} %ow_h.1, bf16[4,2048]{1,0:T(4,128)(2,1)} %bitcast.15, ...), custom_call_target="tpu_custom_call" | custom-call | tf_op jit(solution)/shard_map/layer/pallas_call | solution.py:737
  56.2 1.3 %copy.24 = bf16[128,16]{0,1:T(8,128)(2,1)} copy(bf16[128,16]{0,1:T(8,128)(2,1)} %bitcast.17) | data formatting | bytes 8192

commit v4 on v1

v4 whole, which is shorter than its diff:
```python
import functools

import jax
import jax.numpy as jnp
from jax import lax
from jax.experimental import pallas as pl
from jax.experimental.pallas import tpu as pltpu
from jax.sharding import PartitionSpec as P

EPS = 1e-06
MESH = pl.DeviceIdType.MESH
F32 = jnp.float32
BF16 = jnp.bfloat16
KINDS = 4
ROWS = 40
HIDDEN_PAD = 48


def ring_order(n):
    return sorted(range(1, n), key=lambda d: (-min(d, n - d), d))


def dot(a, b, ca=1, cb=0, precision=None):
    return lax.dot_general(
        a, b, (((ca,), (cb,)), ((), ())), preferred_element_type=F32, precision=precision
    )


def iota(shape, dim):
    return lax.broadcasted_iota(jnp.int32, shape, dim)


def kernel(
    n,
    tok_h,
    pre_h,
    qw_h,
    kw_h,
    vw_h,
    ow_h,
    ig_h,
    fg_h,
    ck_h,
    cv_h,
    ci_h,
    cf_h,
    len_h,
    sm_h,
    sn_h,
    smax_h,
    hg_h,
    mixw_h,
    mg_h,
    gw_h,
    uw_h,
    dw_h,
    out_ref,
    tok,
    pre,
    w4,
    gates,
    cfi,
    lens,
    smax,
    state,
    sn,
    ckv,
    hg,
    mixw,
    mg,
    gud,
    load_sem,
    p1,
    r1,
    relay,
    merged,
    q2f,
    q2b,
    r2,
    split,
    pick,
    mh,
    wg,
    tg,
    rbuf,
    rt,
    gu,
    dt,
    xo,
    xi,
    p5,
    p5b,
    r3,
    result,
    s1,
    v1,
    sr,
    vr,
    s2,
    v2,
    sw,
    vw,
    st,
    vt,
    s3,
    v3,
    s5,
    v5,
    s6,
    v6,
    s7,
    v7,
    s8,
    v8,
    s9,
):
    kvs = n * n
    width = tok.shape[0]
    seqs = tok.shape[1]
    cols = w4.shape[2]
    wide = p1.shape[2]
    blocks = cols // 128
    model = width * kvs
    dp = lax.axis_index("dp")
    kv = lax.axis_index("kv")
    tp = lax.axis_index("tp")
    z, y = kv // n, kv % n
    far = n - (n - 1) * tp
    near = 1 + (n - 1) * tp
    first = z + (y - z) * tp
    second = y + (z - y) * tp
    other = 1 - tp
    order = ring_order(n)

    def first_peer(d):
        return (dp, lax.rem(first + d, n) * far + second * near, tp)

    def second_peer(d):
        return (dp, first * far + lax.rem(second + d, n) * near, tp)

    sibling = (dp, kv, other)

    loads = [
        (tok_h, tok, 0),
        (pre_h, pre, 1),
        (qw_h, w4.at[0], 2),
        (kw_h, w4.at[1], 2),
        (vw_h, w4.at[2], 2),
        (ow_h, w4.at[3], 2),
        (ig_h, gates.at[0], 3),
        (fg_h, gates.at[1], 3),
        (cf_h, cfi.at[0], 4),
        (ci_h, cfi.at[1], 4),
        (len_h, lens, 5),
        (smax_h, smax, 6),
        (sm_h, state, 7),
        (sn_h, sn, 8),
        (ck_h, ckv.at[0], 9),
        (cv_h, ckv.at[1], 9),
        (hg_h, hg, 10),
        (mixw_h, mixw, 11),
        (mg_h, mg, 12),
        (gw_h, gud.at[0], 13),
        (uw_h, gud.at[1], 13),
        (dw_h, gud.at[2], 13),
    ]
    copies = [pltpu.make_async_copy(a, b, load_sem.at[k]) for a, b, k in loads]
    landed = [tok, pre, w4, gates, cfi, lens, smax, state, sn, ckv, hg, mixw, mg, gud]
    arrived = [pltpu.make_async_copy(r, r, load_sem.at[k]) for k, r in enumerate(landed)]
    for c in copies[:8]:
        c.start()
    barrier = pltpu.get_barrier_semaphore()
    for d in range(1, n):
        pl.semaphore_signal(barrier, inc=1, device_id=first_peer(d), device_id_type=MESH)
        pl.semaphore_signal(barrier, inc=1, device_id=second_peer(d), device_id_type=MESH)
        across = (dp, z * n + lax.rem(y + d, n), other)
        pl.semaphore_signal(barrier, inc=1, device_id=across, device_id_type=MESH)
    pl.semaphore_signal(barrier, inc=1, device_id=sibling, device_id_type=MESH)
    for c in copies[8:]:
        c.start()
    for c in arrived[:4]:
        c.wait()

    r = iota((seqs, seqs), 0)
    owner = (r // (2 * n)) * far + (r % n) * near
    perm = jnp.where(iota((seqs, seqs), 1) == owner * 2 + (r // n) % 2, 1.0, 0.0).astype(BF16)
    tokens = dot(perm, tok[...], 1, 1)
    squares = jnp.sum(tokens * tokens, axis=1, keepdims=True)
    normed = (tokens * pre[...]).astype(BF16)
    for k in range(KINDS):
        prod = dot(normed, w4[k]).astype(BF16)
        p1[:, :, k * cols : (k + 1) * cols] = prod.reshape(n, 2 * n, cols)
    lane0 = pl.multiple_of((kv // (128 // width)) * 128, 128)
    both = jnp.concatenate(
        [gates[0, :, pl.ds(lane0, 128)].astype(F32), gates[1, :, pl.ds(lane0, 128)].astype(F32)],
        axis=0,
    ).astype(BF16)
    at = (kv % (128 // width)) * width
    sel = jnp.where(iota((width, 128), 1) == iota((width, 128), 0) + at, 1.0, 0.0).astype(BF16)
    own_gates = dot(both, sel, 1, 1)
    own_gates = jnp.concatenate([own_gates, jnp.zeros((120, width), F32)], axis=0).astype(BF16)
    g = dot(normed, own_gates, 1, 1)
    g = jnp.where(iota((seqs, 128), 1) == 8, squares, g)
    p1[:, :, KINDS * cols :] = g.astype(BF16).reshape(n, 2 * n, 128)

    pl.semaphore_wait(barrier, 3 * (n - 1) + 1)

    def total(ref, send, recv):
        return pltpu.make_async_remote_copy(
            src_ref=ref,
            dst_ref=ref,
            send_sem=send,
            recv_sem=recv,
            device_id=sibling,
            device_id_type=MESH,
        )

    def send(src, dst, send_sem, recv_sem, peer):
        pltpu.make_async_remote_copy(
            src_ref=src,
            dst_ref=dst,
            send_sem=send_sem,
            recv_sem=recv_sem,
            device_id=peer,
            device_id_type=MESH,
        ).start()

    far_d = n // 2
    cut = (KINDS * blocks // 2 + 1) * 128
    parts = (pl.ds(0, cut), pl.ds(cut, wide - cut))

    def rows_for(d):
        return p1.at[lax.rem(first + d, n)]

    hops = (n - 1, 1)
    last_d = (far_d + 1, far_d - 1)
    slot = {d: k for k, d in enumerate(d for d in range(1, n) if d != far_d)}
    for k in range(2):
        part = rows_for(far_d).at[:, parts[k]]
        send(part, relay.at[:, parts[k]], sr, vr.at[k], first_peer(hops[k]))
    for k in range(2):
        d, own_part = last_d[k], parts[1 - k]
        send(rows_for(d).at[:, own_part], r1.at[slot[d], :, own_part], s1, v1, first_peer(d))
    direct = [d for d in order if d != far_d and d not in last_d]
    for d in direct:
        if d not in hops:
            send(rows_for(d), r1.at[slot[d]], s1, v1, first_peer(d))

    for c in arrived[4:]:
        c.wait()
    row64 = iota((8, ckv.shape[2]), 0)
    lane64 = iota((8, ckv.shape[2]), 1)
    zero4 = jnp.zeros((4, ckv.shape[2]), F32)
    forget = jnp.concatenate([cfi[0, 0], cfi[0, 1], zero4], axis=0)
    gain_in = jnp.concatenate([cfi[1, 0], cfi[1, 1], zero4], axis=0)
    length = jnp.where(row64 < 2, lens[0], lens[1])
    live = lane64 < length
    forget = jnp.where(live, forget, 0.0)
    span = ckv.shape[2]
    tri = jnp.where(iota((span, span), 0) <= iota((span, span), 1), 1.0, 0.0)
    running = dot(forget, tri, precision=lax.Precision.HIGHEST)
    run_last = jnp.sum(forget, axis=1, keepdims=True)
    base = jnp.where(live, run_last - running + gain_in, -jnp.inf)
    base = jnp.where(row64 < 4, base, 0.0)
    base_max = jnp.max(base, axis=1, keepdims=True)
    row1 = iota((8, 1), 0)
    state_top = jnp.where(
        row1 == 0,
        smax[0, 0],
        jnp.where(row1 == 1, smax[0, 1], jnp.where(row1 == 2, smax[1, 0], smax[1, 1])),
    )
    state_base = run_last + state_top
    for i in range(2):
        for h in range(2):
            whole = state[i, h]
            high = whole.astype(BF16)
            split[0, 2 * i + h] = high
            split[1, 2 * i + h] = (whole - high.astype(F32)).astype(BF16)
    size = sn.shape[2]
    zero_rows = jnp.zeros((4, size), F32)
    norm8 = jnp.concatenate([sn[0], sn[1], zero_rows], axis=0)
    halves = [hg[:, :size], hg[:, size:]]
    gain8 = jnp.concatenate(halves + halves + [zero_rows], axis=0)
    pr = iota((8 * n, 8 * n), 0)
    pc = iota((8 * n, 8 * n), 1)
    seq, hu = pr % (2 * n), pr // (2 * n)
    target = (seq // 2) * 8 + (hu % 2) * 4 + (seq % 2) * 2 + hu // 2
    pick[...] = jnp.where(pc == target, 1.0, 0.0).astype(BF16)
    hidden_cols = gud.shape[1]
    line = n * width
    c1 = iota((line, line), 1)
    source = ((c1 % (line // 2)) // (width // 2)) * width
    source = source + (c1 // (line // 2)) * (width // 2) + c1 % (width // 2)
    compress = jnp.where(iota((line, line), 0) == source, 1.0, 0.0).astype(BF16)
    pad = jnp.zeros((HIDDEN_PAD - hidden_cols, line), F32)
    for k in range(n):
        at = slice(k * line, (k + 1) * line)
        gain = mg[:, at]
        block = [(gud[u, :, at].astype(F32) * gain) for u in range(2)]
        block = jnp.concatenate([block[0], pad, block[1], pad], axis=0).astype(BF16)
        block = dot(block, compress).astype(BF16)
        for u in range(2):
            to = (u * n + k) * (line // 2)
            gu[:, to : to + line // 2] = block[:, u * (line // 2) : (u + 1) * (line // 2)]
    group = 128 // width

    def arrange(b, carry):
        block = gud[2, :, pl.ds(pl.multiple_of(b * 128, 128), 128)].astype(F32)
        block = jnp.concatenate([block, jnp.zeros((HIDDEN_PAD - hidden_cols, 128), F32)], axis=0)
        block = block.T.astype(BF16)
        for k in range(group):
            at_kv = b * group + k
            mirrored = (at_kv % n) * n + at_kv // n
            half = width // 2
            dt[0, at_kv] = block[k * width : k * width + half]
            dt[1, mirrored] = block[k * width + half : (k + 1) * width]
        return carry

    lax.fori_loop(0, kvs // group, arrange, 0)

    for k in range(2):
        d = last_d[k]
        total(relay.at[:, parts[k]], sr, vr.at[k]).wait_recv()
        mine = p1[lax.rem(first + d, n), :, parts[k]].astype(F32)
        merged[:, parts[k]] = (mine + relay[:, parts[k]].astype(F32)).astype(BF16)
        send(merged.at[:, parts[k]], r1.at[slot[d], :, parts[k]], s1, v1, first_peer(d))
    for d in direct:
        if d in hops:
            send(rows_for(d), r1.at[slot[d]], s1, v1, first_peer(d))
    half = width // 2
    own_rows = pl.ds(pl.multiple_of(tp * half, half), half)
    rest = pl.ds(pl.multiple_of(other * half, half), half)

    def share_weights():
        for d in order:
            along_y = z * n + lax.rem(y + d, n)
            send(tok.at[own_rows], tg.at[y], st, vt, (dp, along_y, tp))
            send(mixw.at[own_rows], wg.at[tp, y], sw, vw, (dp, along_y, tp))
            send(mixw.at[rest], wg.at[tp, y], sw, vw, (dp, along_y, other))
        send(mixw.at[rest], wg.at[tp, y], sw, vw, sibling)

    @pl.when(tp == 1)
    def _():
        share_weights()

    own = p1[first].astype(F32)
    total(r1, s1, v1).wait_recv()
    for k in range(n - 2):
        own = own + r1[k].astype(F32)
    q2f[...] = jnp.zeros_like(q2f)
    for i in range(2):
        part = own[i * n : (i + 1) * n]
        for c in range(KINDS * blocks):
            kind, h, u = c // blocks, (c % blocks) // 2, c % 2
            q2f[pl.ds(kind * 8 + u * 4 + i * 2 + h, n, stride=ROWS), :] = part[
                :, c * 128 : (c + 1) * 128
            ]
        for h in range(2):
            q2f[pl.ds(32 + i * 2 + h, n, stride=ROWS), :] = part[:, KINDS * cols :]
    q2b[...] = q2f[...].reshape(n, ROWS, 128).astype(BF16)
    for d in order:
        send(q2b.at[lax.rem(second + d, n)], r2.at[d - 1], s2, v2, second_peer(d))
    @pl.when(tp == 0)
    def _():
        share_weights()

    wg[tp, y] = mixw[own_rows, :]
    tg[y] = tok[own_rows, :]
    mine = q2f[pl.ds(pl.multiple_of(second * ROWS, 8), ROWS), :]
    total(r2, s2, v2).wait_recv()
    for k in range(n - 1):
        mine = mine + r2[k].astype(F32)

    def heads(kind):
        a = mine[kind * 8 : kind * 8 + 4]
        b = mine[kind * 8 + 4 : kind * 8 + 8]
        return jnp.concatenate([jnp.concatenate([a, b], axis=1), zero_rows], axis=0)

    gate8 = mine[32:40]
    lane = iota((8, 128), 1)
    row = iota((8, 128), 0)
    square = jnp.sum(jnp.where(lane == 8, gate8, 0.0), axis=1, keepdims=True)
    in_sum = jnp.sum(jnp.where(lane == 2 * tp + row % 2, gate8, 0.0), axis=1, keepdims=True)
    fg_sum = jnp.sum(jnp.where(lane == 4 + 2 * tp + row % 2, gate8, 0.0), axis=1, keepdims=True)
    scale = lax.rsqrt(square / model + EPS)
    query = (scale * heads(0)).astype(BF16).astype(F32)
    key_new = (scale * heads(1)).astype(BF16).astype(F32)
    value_new = (scale * heads(2)).astype(BF16).astype(F32)
    outgate = (scale * heads(3)).astype(BF16).astype(F32)
    in_gate = scale * in_sum
    fg = scale * fg_sum
    forget_new = jnp.minimum(fg, 0.0) - jnp.log1p(jnp.exp(-jnp.abs(fg)))
    weight_log = base + forget_new
    state_log = state_base + forget_new
    peak = jnp.maximum(jnp.maximum(state_log, in_gate), base_max + forget_new)
    query = query * (size**-0.5)
    rows = iota((8, size), 0)
    alone = [jnp.where(rows == k, query, 0.0) for k in range(4)]
    dots = dot(jnp.concatenate(alone[0:2], axis=1).astype(BF16), ckv[0, 0], 1, 1)
    dots = dots + dot(jnp.concatenate(alone[2:4], axis=1).astype(BF16), ckv[0, 1], 1, 1)
    scores = jnp.exp(weight_log - peak) * dots
    self_score = jnp.exp(in_gate - peak) * jnp.sum(query * key_new, axis=1, keepdims=True)
    carried = jnp.exp(state_log - peak)
    read = dot(alone[0].astype(BF16), split[0, 0], 1, 1)
    read = read + dot(alone[0].astype(BF16), split[1, 0], 1, 1)
    for k in range(1, 4):
        read = read + dot(alone[k].astype(BF16), split[0, k], 1, 1)
        read = read + dot(alone[k].astype(BF16), split[1, k], 1, 1)
    norm_read = jnp.sum(norm8 * query, axis=1, keepdims=True)
    values = dot(jnp.where(row64 < 2, scores, 0.0).astype(BF16), ckv[1, 0])
    values = values + dot(jnp.where(row64 >= 2, scores, 0.0).astype(BF16), ckv[1, 1])
    values = jnp.where(rows % 2 == 0, values[:, :size], values[:, size:])
    numerator = carried * read + values + self_score * value_new
    denominator = carried * norm_read + jnp.sum(scores, axis=1, keepdims=True) + self_score
    hidden = numerator / jnp.maximum(jnp.abs(denominator), 1.0)
    mixed = hidden * gain8 * jax.nn.sigmoid(outgate)
    mh[tp, z] = jnp.concatenate([mixed[:4, :128], mixed[:4, 128:]], axis=0).astype(BF16)

    for d in order:
        along_z = lax.rem(z + d, n) * n + y
        for core in (tp, other):
            send(mh.at[tp, z], mh.at[tp, z], s3, v3, (dp, along_z, core))
    send(mh.at[tp, z], mh.at[tp, z], s3, v3, sibling)
    flat_w = wg.reshape(2 * n, half, cols)
    flat_m = mh.reshape(2 * n, 8, 128)
    all_wg = total(flat_w.at[pl.ds(0, 2 * n - 1)], sw, vw)
    all_tg = total(tg.at[pl.ds(0, n - 1)], st, vt)
    all_mh = total(flat_m.at[pl.ds(0, 2 * n - 1)], s3, v3)
    for c in (all_wg, all_tg, all_mh):
        c.wait_recv()

    def project(u):
        flat = mh[u].astype(F32).reshape(8 * n, 128).astype(BF16)
        picked = dot(pick[...], flat).astype(BF16)
        w = wg[u].reshape(n * half, cols)
        out = dot(picked[: 2 * n], w[:, :128], 1, 1)
        for k in range(1, 4):
            block = picked[2 * n * k : 2 * n * (k + 1)]
            out = out + dot(block, w[:, k * 128 : (k + 1) * 128], 1, 1)
        return out.astype(BF16).astype(F32)

    q = iota((2 * n, seqs), 0)
    here = jnp.where(iota((2 * n, seqs), 1) == ((q // 2) * n + y) * 2 + q % 2, 1.0, 0.0)
    own_tokens = dot(here.astype(BF16), tg[...].reshape(n * half, seqs), 1, 1)
    rbuf[...] = (own_tokens + (project(0) + project(1))).astype(BF16)

    rt[tp, z, y] = rbuf[...]
    rows_order = order + [0]
    for dz in rows_order:
        for dy in rows_order:
            if dz or dy:
                peer = lax.rem(z + dz, n) * n + lax.rem(y + dy, n)
                send(rbuf, rt.at[tp, z, y], s5, v5.at[dz], (dp, peer, tp))
    for dz in rows_order:
        count = n if dz else n - 1
        total(rt.at[0, 0, pl.ds(0, count)], s5, v5.at[dz]).wait_recv()
        source = lax.rem(z + n - dz, n)
        send(rt.at[tp, source], rt.at[tp, source], s6, v6, sibling)
    total(rt.at[0], s6, v6).wait_recv()

    lanes = n * half
    power = jnp.zeros((seqs, lanes), F32)
    acc = jnp.zeros((2 * HIDDEN_PAD, seqs), F32)
    for u in range(2):
        for k in range(0, n, 2):
            pair = [rt[u, k + e].reshape(seqs, lanes) for e in range(2)]
            at = (u * n + k) * lanes
            wide_pair = jnp.concatenate(pair, axis=1)
            acc = acc + dot(gu[:, at : at + 2 * lanes], wide_pair, 1, 1)
            for block in pair:
                spread = block.astype(F32)
                power = power + spread * spread
    power = dot(jnp.ones((8, lanes), F32), power, 1, 1, precision=lax.Precision.HIGHEST)[:1]
    scale_mid = lax.rsqrt(power / model + EPS)
    gate = scale_mid * acc[:HIDDEN_PAD]
    up = scale_mid * acc[HIDDEN_PAD:]
    units = (gate * jax.nn.sigmoid(gate) * up).astype(BF16)

    other_first = y + (z - y) * tp
    steps = order + [0]
    whole = dot(dt[other].reshape(kvs * half, HIDDEN_PAD), units)
    xo[...] = whole.astype(BF16).reshape(n, n * half, seqs)
    for k, d in enumerate(steps):
        send(xo.at[lax.rem(other_first + d, n)], xi.at[k], s7, v7.at[k], sibling)
    p5[...] = dot(dt[tp].reshape(kvs * half, HIDDEN_PAD), units).reshape(n, n * half, seqs)
    for k, d in enumerate(steps):
        total(xi.at[k], s7, v7.at[k]).wait_recv()
        at_f = lax.rem(first + d, n)
        both = p5[at_f] + xi[k].astype(F32)
        p5b[k] = both.astype(BF16).reshape(n, half, seqs)
        if d == 0:
            p5[at_f] = both
        for e in steps:
            if d or e:
                at_s = lax.rem(second + e, n)
                peer = (dp, at_f * far + at_s * near, tp)
                send(p5b.at[k, at_s], r3.at[d * n + e - 1], s8, v8, peer)
    mine_at = jnp.where(iota((half, lanes), 1) == iota((half, lanes), 0) + y * half, 1.0, 0.0)
    last = dot(mine_at.astype(BF16), rt[tp, z].reshape(seqs, lanes), 1, 1)
    last = last + p5[first, pl.ds(pl.multiple_of(second * half, half), half), :]
    c2 = iota((seqs, seqs), 1)
    back = ((c2 // 2) % n) * 2 * n + (c2 // (2 * n)) * 2 + c2 % 2
    back = jnp.where(iota((seqs, seqs), 0) == back, 1.0, 0.0).astype(BF16)
    total(r3, s8, v8).wait_recv()
    last = last + jnp.sum(r3[...].astype(F32), axis=0)
    result[...] = dot(last.astype(BF16), back).astype(BF16)
    written = pltpu.make_async_copy(result, out_ref, s9)
    written.start()

    total(relay, sr, vr.at[0]).wait_send()
    total(r1, s1, v1).wait_send()
    total(r2, s2, v2).wait_send()
    for c in (all_wg, all_tg, all_mh):
        c.wait_send()
    flat_r = rt.reshape(2 * kvs, 2 * n, lanes)
    total(flat_r.at[pl.ds(0, kvs - 1)], s5, v5.at[0]).wait_send()
    total(rt.at[0], s6, v6).wait_send()
    total(xi, s7, v7.at[0]).wait_send()
    total(r3, s8, v8).wait_send()
    written.wait()


def per_device(n, *args):
    (tokens, pre, qw, kw, vw, ow, ig, fg, ck, cv, ci, cf, lens, sm, sn, smax) = args[:16]
    hg, mixw, mg, gw, uw, dw = args[16:]
    operands = (
        tokens.T,
        pre.reshape(1, -1),
        qw,
        kw,
        vw,
        ow,
        ig.T,
        fg.T,
        ck,
        cv,
        ci.transpose(0, 2, 1),
        cf.transpose(0, 2, 1),
        lens,
        sm,
        sn,
        smax,
        hg.reshape(1, -1),
        mixw.T,
        mg.reshape(1, -1),
        gw.T,
        uw.T,
        dw,
    )
    seqs, width = tokens.shape
    cols = qw.shape[1]
    kvs = n * n
    model = width * kvs
    span, size = ck.shape[1], sn.shape[2]
    wide = KINDS * cols + 128
    half = width // 2
    dma = pltpu.SemaphoreType.DMA
    vmem = pltpu.VMEM
    ff = gw.shape[1]
    scratch = [
        vmem((width, seqs), BF16),
        vmem((1, width), F32),
        vmem((KINDS, width, cols), BF16),
        vmem((2, 4, model), BF16),
        vmem((2, 2, 2, span), F32),
        pltpu.SMEM((2,), jnp.int32),
        pltpu.SMEM((2, 2), F32),
        vmem((2, 2, size, size), F32),
        vmem((2, 2, size), F32),
        vmem((2, 2, span, cols), BF16),
        vmem((1, cols), F32),
        vmem((width, cols), BF16),
        vmem((1, model), F32),
        vmem((3, ff, model), BF16),
        dma((14,)),
        vmem((n, 2 * n, wide), BF16),
        vmem((n - 2, 2 * n, wide), BF16),
        vmem((2 * n, wide), BF16),
        vmem((2 * n, wide), BF16),
        vmem((n * ROWS, 128), F32),
        vmem((n, ROWS, 128), BF16),
        vmem((n - 1, ROWS, 128), BF16),
        vmem((2, 4, size, size), BF16),
        vmem((8 * n, 8 * n), BF16),
        vmem((2, n, 8, 128), BF16),
        vmem((2, n, half, cols), BF16),
        vmem((n, half, seqs), BF16),
        vmem((2 * n, n * half), BF16),
        vmem((2, n, n, 2 * n, n * half), BF16),
        vmem((2 * HIDDEN_PAD, model), BF16),
        vmem((2, kvs, half, HIDDEN_PAD), BF16),
        vmem((n, n * half, seqs), BF16),
        vmem((n, n * half, seqs), BF16),
        vmem((n, n * half, seqs), F32),
        vmem((n, n, half, seqs), BF16),
        vmem((kvs - 1, half, seqs), BF16),
        vmem((half, seqs), BF16),
        dma,
        dma,
        dma,
        dma((2,)),
        dma,
        dma,
        dma,
        dma,
        dma,
        dma,
        dma,
        dma,
        dma,
        dma((n,)),
        dma,
        dma,
        dma,
        dma((n,)),
        dma,
        dma,
        dma,
    ]
    out = pl.pallas_call(
        functools.partial(kernel, n),
        out_shape=jax.ShapeDtypeStruct((half, seqs), BF16),
        in_specs=[pl.BlockSpec(memory_space=pl.ANY)] * len(operands),
        out_specs=pl.BlockSpec(memory_space=pl.ANY),
        scratch_shapes=scratch,
        compiler_params=pltpu.CompilerParams(
            collective_id=0, has_side_effects=True, vmem_limit_bytes=62 * 1024 * 1024
        ),
        name="layer",
    )(*operands)
    return out.T


def solution(mesh):
    n = round(mesh.shape["kv"] ** 0.5)
    seq = ("dp", "kv")
    return jax.shard_map(
        functools.partial(per_device, n),
        mesh=mesh,
        in_specs=(
            P("dp", "kv"),
            P("kv"),
            P("kv", "tp"),
            P("kv", "tp"),
            P("kv", "tp"),
            P("kv", "tp"),
            P(),
            P(),
            P(seq, None, "tp"),
            P(seq, None, "tp"),
            P(seq, None, "tp"),
            P(seq, None, "tp"),
            P(seq),
            P(seq, "tp", None, None),
            P(seq, "tp", None),
            P(seq, "tp"),
            P("tp"),
            P("tp", "kv"),
            P(),
            P(None, ("kv", "tp")),
            P(None, ("kv", "tp")),
            P(("kv", "tp"), None),
        ),
        out_specs=P("dp", ("kv", "tp")),
        check_vma=False,
    )
```

time: 62.8 us -> 57.4 us (0.914)
  Pallas kernels: 60.9 us -> 55.9 us
    pallas_call x1, Pallas kernels: 60.9 us -> 55.9 us  [per_device(): pl.pallas_call(functools.partial(kernel, n), out_shape=jax.ShapeDtypeStru...]
where the time goes in v4:
time: 57.4 us; the launch traced here: 57.2 us
  Pallas kernels  55.9 us (97%)
  local copies, waits for them, and re-layouts  1.28 us (2%)
    pallas_call x1, Pallas kernels, per_device(): pl.pallas_call(functools.partial(kernel, n), out_shape=jax.ShapeDtypeStru...  55.9 us
    unnamed x1, local copies, waits for them, and re-layouts  1.28 us

profile of v4, /device:TPU:1, one launch (start us, length us, event | category | flops | bytes accessed | tf_op | source)
XLA Modules:
  0.0 57.2 jit_solution(6504857432346209590)
XLA Ops:
  0.0 55.9 %layer.1 = bf16[16,128]{1,0:T(8,128)(2,1)} custom-call(bf16[32,128]{1,0:T(8,128)(2,1)} %bitcast.18, f32[1,32]{1,0:T(1,128)} %bitcast.23, bf16[32,512]{1,0:T(8,128)(2,1)} %qw_h.1, bf16[32,512]{1,0:T(8,128)(2,1)} %kw_h.1, bf16[32,512]{1,0:T(8,128)(2,1)} %vw_h.1, bf16[32,512]{1,0:T(8,128)(2,1)} %ow_h.1, bf16[4,2048]{1,0:T(4,128)(2,1)} %bitcast.15, ...), custom_call_target="tpu_custom_call" | custom-call | tf_op jit(solution)/shard_map/layer/pallas_call | solution.py:620
  56.0 1.3 %copy.24 = bf16[128,16]{0,1:T(8,128)(2,1)} copy(bf16[128,16]{0,1:T(8,128)(2,1)} %bitcast.17) | data formatting | bytes 8192

commit v5 on v4

--- a/solution.py
+++ b/solution.py
@@ -91,7 +91,6 @@
     p5,
     p5b,
     r3,
-    result,
     s1,
     v1,
     sr,
@@ -112,7 +111,6 @@
     v7,
     s8,
     v8,
-    s9,
 ):
     kvs = n * n
     width = tok.shape[0]
@@ -503,9 +501,7 @@
     back = jnp.where(iota((seqs, seqs), 0) == back, 1.0, 0.0).astype(BF16)
     total(r3, s8, v8).wait_recv()
     last = last + jnp.sum(r3[...].astype(F32), axis=0)
-    result[...] = dot(last.astype(BF16), back).astype(BF16)
-    written = pltpu.make_async_copy(result, out_ref, s9)
-    written.start()
+    out_ref[...] = dot(last.astype(BF16), back).astype(BF16)
 
     total(relay, sr, vr.at[0]).wait_send()
     total(r1, s1, v1).wait_send()
@@ -517,7 +513,6 @@
     total(rt.at[0], s6, v6).wait_send()
     total(xi, s7, v7.at[0]).wait_send()
     total(r3, s8, v8).wait_send()
-    written.wait()
 
 
 def per_device(n, *args):
@@ -594,7 +589,6 @@
         vmem((n, n * half, seqs), F32),
         vmem((n, n, half, seqs), BF16),
         vmem((kvs - 1, half, seqs), BF16),
-        vmem((half, seqs), BF16),
         dma,
         dma,
         dma,
@@ -613,7 +607,6 @@
         dma,
         dma,
         dma((n,)),
-        dma,
         dma,
         dma,
     ]
@@ -621,13 +614,13 @@
         functools.partial(kernel, n),
         out_shape=jax.ShapeDtypeStruct((half, seqs), BF16),
         in_specs=[pl.BlockSpec(memory_space=pl.ANY)] * len(operands),
-        out_specs=pl.BlockSpec(memory_space=pl.ANY),
+        out_specs=pl.BlockSpec(memory_space=pltpu.VMEM),
         scratch_shapes=scratch,
         compiler_params=pltpu.CompilerParams(
-            collective_id=0, has_side_effects=True, vmem_limit_bytes=62 * 1024 * 1024
+            collective_id=0, has_side_effects=True, vmem_limit_bytes=24 * 1024 * 1024
         ),
         name="layer",
-    )(*operands)
+    )(*[pltpu.with_memory_space_constraint(o, pltpu.HBM) for o in operands])
     return out.T
 
 

time: 57.4 us -> 56.1 us (0.977)
  local copies, waits for them, and re-layouts: 1.28 us -> 0.6 us
    unnamed x1, local copies, waits for them, and re-layouts: 1.28 us -> 0.6 us
    pallas_call x1, Pallas kernels: 55.9 us -> 55.4 us  [per_device(): pl.pallas_call(functools.partial(kernel, n), out_shape=jax.ShapeDtypeStru...]
where the time goes in v5:
time: 56.1 us; the launch traced here: 56 us
  Pallas kernels  55.4 us (99%)
  local copies, waits for them, and re-layouts  0.6 us (1%)
    pallas_call x1, Pallas kernels, per_device(): pl.pallas_call(functools.partial(kernel, n), out_shape=jax.ShapeDtypeStru...  55.4 us

profile of v5, /device:TPU:1, one launch (start us, length us, event | category | flops | bytes accessed | tf_op | source)
XLA Modules:
  0.0 56.0 jit_solution(1998040708549398932)
XLA Ops:
  0.0 55.4 %layer.1 = bf16[16,128]{1,0:T(8,128)(2,1)S(1)} custom-call(bf16[32,128]{1,0:T(8,128)(2,1)} %bitcast.18, f32[1,32]{1,0:T(1,128)} %bitcast.23, bf16[32,512]{1,0:T(8,128)(2,1)} %qw_h.1, bf16[32,512]{1,0:T(8,128)(2,1)} %kw_h.1, bf16[32,512]{1,0:T(8,128)(2,1)} %vw_h.1, bf16[32,512]{1,0:T(8,128)(2,1)} %ow_h.1, bf16[4,2048]{1,0:T(4,128)(2,1)} %bitcast.16, ...), custom_call_target="tpu_custom_call" | custom-call | tf_op jit(solution)/shard_map/layer/pallas_call | solution.py:613
  55.4 0.6 %copy.24 = bf16[128,16]{0,1:T(8,128)(2,1)} copy(bf16[128,16]{0,1:T(8,128)(2,1)S(1)} %bitcast.12) | data formatting | bytes 8192

commit v6 on v5

--- a/solution.py
+++ b/solution.py
@@ -86,8 +86,8 @@
     rt,
     gu,
     dt,
-    xo,
-    xi,
+    dts,
+    dtc,
     p5,
     p5b,
     r3,
@@ -107,8 +107,10 @@
     v5,
     s6,
     v6,
-    s7,
-    v7,
+    sg,
+    vg,
+    sd,
+    vd,
     s8,
     v8,
 ):
@@ -299,7 +301,7 @@
         block = dot(block, compress).astype(BF16)
         for u in range(2):
             to = (u * n + k) * (line // 2)
-            gu[:, to : to + line // 2] = block[:, u * (line // 2) : (u + 1) * (line // 2)]
+            gu[tp, :, to : to + line // 2] = block[:, u * (line // 2) : (u + 1) * (line // 2)]
     group = 128 // width
 
     def arrange(b, carry):
@@ -315,6 +317,8 @@
         return carry
 
     lax.fori_loop(0, kvs // group, arrange, 0)
+    send(gu.at[tp], gu.at[tp], sg, vg, sibling)
+    send(dt.at[other], dts, sd, vd, sibling)
 
     for k in range(2):
         d = last_d[k]
@@ -364,6 +368,10 @@
 
     wg[tp, y] = mixw[own_rows, :]
     tg[y] = tok[own_rows, :]
+    total(dts, sd, vd).wait_recv()
+    half_dt = [dt[tp].reshape(kvs * half, HIDDEN_PAD), dts[...].reshape(kvs * half, HIDDEN_PAD)]
+    half_dt = [jnp.where(tp == c, half_dt[0], half_dt[1]) for c in range(2)]
+    dtc[...] = jnp.concatenate(half_dt, axis=1)
     mine = q2f[pl.ds(pl.multiple_of(second * ROWS, 8), ROWS), :]
     total(r2, s2, v2).wait_recv()
     for k in range(n - 1):
@@ -458,41 +466,39 @@
 
     lanes = n * half
     power = jnp.zeros((seqs, lanes), F32)
-    acc = jnp.zeros((2 * HIDDEN_PAD, seqs), F32)
+    acc = jnp.zeros((4 * HIDDEN_PAD, seqs), F32)
+    total(gu.at[0], sg, vg).wait_recv()
     for u in range(2):
         for k in range(0, n, 2):
             pair = [rt[u, k + e].reshape(seqs, lanes) for e in range(2)]
             at = (u * n + k) * lanes
             wide_pair = jnp.concatenate(pair, axis=1)
-            acc = acc + dot(gu[:, at : at + 2 * lanes], wide_pair, 1, 1)
+            both = gu[:, :, at : at + 2 * lanes].reshape(4 * HIDDEN_PAD, 2 * lanes)
+            acc = acc + dot(both, wide_pair, 1, 1)
             for block in pair:
                 spread = block.astype(F32)
                 power = power + spread * spread
     power = dot(jnp.ones((8, lanes), F32), power, 1, 1, precision=lax.Precision.HIGHEST)[:1]
     scale_mid = lax.rsqrt(power / model + EPS)
-    gate = scale_mid * acc[:HIDDEN_PAD]
-    up = scale_mid * acc[HIDDEN_PAD:]
-    units = (gate * jax.nn.sigmoid(gate) * up).astype(BF16)
-
-    other_first = y + (z - y) * tp
+    acc = scale_mid * acc
+    units = []
+    for c in range(2):
+        gate = acc[2 * c * HIDDEN_PAD : (2 * c + 1) * HIDDEN_PAD]
+        up = acc[(2 * c + 1) * HIDDEN_PAD : (2 * c + 2) * HIDDEN_PAD]
+        units.append(gate * jax.nn.sigmoid(gate) * up)
+    units = jnp.concatenate(units, axis=0).astype(BF16)
+
     steps = order + [0]
-    whole = dot(dt[other].reshape(kvs * half, HIDDEN_PAD), units)
-    xo[...] = whole.astype(BF16).reshape(n, n * half, seqs)
-    for k, d in enumerate(steps):
-        send(xo.at[lax.rem(other_first + d, n)], xi.at[k], s7, v7.at[k], sibling)
-    p5[...] = dot(dt[tp].reshape(kvs * half, HIDDEN_PAD), units).reshape(n, n * half, seqs)
-    for k, d in enumerate(steps):
-        total(xi.at[k], s7, v7.at[k]).wait_recv()
+    sums = dot(dtc[...], units)
+    p5b[...] = sums.astype(BF16).reshape(n, n, half, seqs)
+    p5[...] = sums.reshape(n, n * half, seqs)
+    for d in steps:
         at_f = lax.rem(first + d, n)
-        both = p5[at_f] + xi[k].astype(F32)
-        p5b[k] = both.astype(BF16).reshape(n, half, seqs)
-        if d == 0:
-            p5[at_f] = both
         for e in steps:
             if d or e:
                 at_s = lax.rem(second + e, n)
                 peer = (dp, at_f * far + at_s * near, tp)
-                send(p5b.at[k, at_s], r3.at[d * n + e - 1], s8, v8, peer)
+                send(p5b.at[at_f, at_s], r3.at[d * n + e - 1], s8, v8, peer)
     mine_at = jnp.where(iota((half, lanes), 1) == iota((half, lanes), 0) + y * half, 1.0, 0.0)
     last = dot(mine_at.astype(BF16), rt[tp, z].reshape(seqs, lanes), 1, 1)
     last = last + p5[first, pl.ds(pl.multiple_of(second * half, half), half), :]
@@ -511,7 +517,8 @@
     flat_r = rt.reshape(2 * kvs, 2 * n, lanes)
     total(flat_r.at[pl.ds(0, kvs - 1)], s5, v5.at[0]).wait_send()
     total(rt.at[0], s6, v6).wait_send()
-    total(xi, s7, v7.at[0]).wait_send()
+    total(gu.at[0], sg, vg).wait_send()
+    total(dts, sd, vd).wait_send()
     total(r3, s8, v8).wait_send()
 
 
@@ -582,10 +589,10 @@
         vmem((n, half, seqs), BF16),
         vmem((2 * n, n * half), BF16),
         vmem((2, n, n, 2 * n, n * half), BF16),
-        vmem((2 * HIDDEN_PAD, model), BF16),
+        vmem((2, 2 * HIDDEN_PAD, model), BF16),
         vmem((2, kvs, half, HIDDEN_PAD), BF16),
-        vmem((n, n * half, seqs), BF16),
-        vmem((n, n * half, seqs), BF16),
+        vmem((kvs, half, HIDDEN_PAD), BF16),
+        vmem((kvs * half, 2 * HIDDEN_PAD), BF16),
         vmem((n, n * half, seqs), F32),
         vmem((n, n, half, seqs), BF16),
         vmem((kvs - 1, half, seqs), BF16),
@@ -606,7 +613,9 @@
         dma,
         dma,
         dma,
-        dma((n,)),
+        dma,
+        dma,
+        dma,
         dma,
         dma,
     ]

time: 56.1 us -> 55.9 us (level)
  no operation moved by 1% of the time
where the time goes in v6:
time: 55.9 us; the launch traced here: 55.8 us
  Pallas kernels  55.2 us (99%)
  local copies, waits for them, and re-layouts  0.6 us (1%)
    pallas_call x1, Pallas kernels, per_device(): pl.pallas_call(functools.partial(kernel, n), out_shape=jax.ShapeDtypeStru...  55.2 us

profile of v6, /device:TPU:1, one launch (start us, length us, event | category | flops | bytes accessed | tf_op | source)
XLA Modules:
  0.0 55.8 jit_solution(10598522093801280856)
XLA Ops:
  0.0 55.2 %layer.1 = bf16[16,128]{1,0:T(8,128)(2,1)S(1)} custom-call(bf16[32,128]{1,0:T(8,128)(2,1)} %bitcast.18, f32[1,32]{1,0:T(1,128)} %bitcast.23, bf16[32,512]{1,0:T(8,128)(2,1)} %qw_h.1, bf16[32,512]{1,0:T(8,128)(2,1)} %kw_h.1, bf16[32,512]{1,0:T(8,128)(2,1)} %vw_h.1, bf16[32,512]{1,0:T(8,128)(2,1)} %ow_h.1, bf16[4,2048]{1,0:T(4,128)(2,1)} %bitcast.16, ...), custom_call_target="tpu_custom_call" | custom-call | tf_op jit(solution)/shard_map/layer/pallas_call | solution.py:622
  55.2 0.6 %copy.24 = bf16[128,16]{0,1:T(8,128)(2,1)} copy(bf16[128,16]{0,1:T(8,128)(2,1)S(1)} %bitcast.12) | data formatting | bytes 8192

commit v7 on v6

--- a/solution.py
+++ b/solution.py
@@ -492,13 +492,12 @@
     sums = dot(dtc[...], units)
     p5b[...] = sums.astype(BF16).reshape(n, n, half, seqs)
     p5[...] = sums.reshape(n, n * half, seqs)
-    for d in steps:
-        at_f = lax.rem(first + d, n)
-        for e in steps:
-            if d or e:
-                at_s = lax.rem(second + e, n)
-                peer = (dp, at_f * far + at_s * near, tp)
-                send(p5b.at[at_f, at_s], r3.at[d * n + e - 1], s8, v8, peer)
+    for dz, dy in sorted([(a, b) for a in steps for b in steps], key=lambda p: -min(p[0], n - p[0]) - min(p[1], n - p[1])):
+        if dz or dy:
+            to_z, to_y = lax.rem(z + dz, n), lax.rem(y + dy, n)
+            at_f, at_s = to_z + (to_y - to_z) * tp, to_y + (to_z - to_y) * tp
+            peer = (dp, to_z * n + to_y, tp)
+            send(p5b.at[at_f, at_s], r3.at[dz * n + dy - 1], s8, v8, peer)
     mine_at = jnp.where(iota((half, lanes), 1) == iota((half, lanes), 0) + y * half, 1.0, 0.0)
     last = dot(mine_at.astype(BF16), rt[tp, z].reshape(seqs, lanes), 1, 1)
     last = last + p5[first, pl.ds(pl.multiple_of(second * half, half), half), :]

time: 55.9 us -> 55.8 us (level)
  no operation moved by 1% of the time
where the time goes in v7:
time: 55.8 us; the launch traced here: 55.6 us
  Pallas kernels  55 us (99%)
  local copies, waits for them, and re-layouts  0.6 us (1%)
    pallas_call x1, Pallas kernels, per_device(): pl.pallas_call(functools.partial(kernel, n), out_shape=jax.ShapeDtypeStru...  55 us

profile of v7, /device:TPU:1, one launch (start us, length us, event | category | flops | bytes accessed | tf_op | source)
XLA Modules:
  0.0 55.6 jit_solution(16741680500680629376)
XLA Ops:
  0.0 55.0 %layer.1 = bf16[16,128]{1,0:T(8,128)(2,1)S(1)} custom-call(bf16[32,128]{1,0:T(8,128)(2,1)} %bitcast.18, f32[1,32]{1,0:T(1,128)} %bitcast.23, bf16[32,512]{1,0:T(8,128)(2,1)} %qw_h.1, bf16[32,512]{1,0:T(8,128)(2,1)} %kw_h.1, bf16[32,512]{1,0:T(8,128)(2,1)} %vw_h.1, bf16[32,512]{1,0:T(8,128)(2,1)} %ow_h.1, bf16[4,2048]{1,0:T(4,128)(2,1)} %bitcast.16, ...), custom_call_target="tpu_custom_call" | custom-call | tf_op jit(solution)/shard_map/layer/pallas_call | solution.py:621
  55.0 0.6 %copy.24 = bf16[128,16]{0,1:T(8,128)(2,1)} copy(bf16[128,16]{0,1:T(8,128)(2,1)S(1)} %bitcast.12) | data formatting | bytes 8192

commit v8 on v7

--- a/solution.py
+++ b/solution.py
@@ -452,11 +452,11 @@
 
     rt[tp, z, y] = rbuf[...]
     rows_order = order + [0]
-    for dz in rows_order:
-        for dy in rows_order:
-            if dz or dy:
-                peer = lax.rem(z + dz, n) * n + lax.rem(y + dy, n)
-                send(rbuf, rt.at[tp, z, y], s5, v5.at[dz], (dp, peer, tp))
+    hops_of = lambda p: -min(p[0], n - p[0]) - min(p[1], n - p[1])
+    for dz, dy in sorted([(a, b) for a in rows_order for b in rows_order], key=hops_of):
+        if dz or dy:
+            peer = lax.rem(z + dz, n) * n + lax.rem(y + dy, n)
+            send(rbuf, rt.at[tp, z, y], s5, v5.at[dz], (dp, peer, tp))
     for dz in rows_order:
         count = n if dz else n - 1
         total(rt.at[0, 0, pl.ds(0, count)], s5, v5.at[dz]).wait_recv()

time: 55.8 us -> 55.1 us (0.987)
  Pallas kernels: 55 us -> 54.3 us
    pallas_call x1, Pallas kernels: 55 us -> 54.3 us  [per_device(): pl.pallas_call(functools.partial(kernel, n), out_shape=jax.ShapeDtypeStru...]
where the time goes in v8:
time: 55.1 us; the launch traced here: 54.9 us
  Pallas kernels  54.3 us (99%)
  local copies, waits for them, and re-layouts  0.6 us (1%)
    pallas_call x1, Pallas kernels, per_device(): pl.pallas_call(functools.partial(kernel, n), out_shape=jax.ShapeDtypeStru...  54.3 us

profile of v8, /device:TPU:1, one launch (start us, length us, event | category | flops | bytes accessed | tf_op | source)
XLA Modules:
  0.0 54.9 jit_solution(15780496878233563387)
XLA Ops:
  0.0 54.3 %layer.1 = bf16[16,128]{1,0:T(8,128)(2,1)S(1)} custom-call(bf16[32,128]{1,0:T(8,128)(2,1)} %bitcast.18, f32[1,32]{1,0:T(1,128)} %bitcast.23, bf16[32,512]{1,0:T(8,128)(2,1)} %qw_h.1, bf16[32,512]{1,0:T(8,128)(2,1)} %kw_h.1, bf16[32,512]{1,0:T(8,128)(2,1)} %vw_h.1, bf16[32,512]{1,0:T(8,128)(2,1)} %ow_h.1, bf16[4,2048]{1,0:T(4,128)(2,1)} %bitcast.16, ...), custom_call_target="tpu_custom_call" | custom-call | tf_op jit(solution)/shard_map/layer/pallas_call | solution.py:621
  54.3 0.6 %copy.24 = bf16[128,16]{0,1:T(8,128)(2,1)} copy(bf16[128,16]{0,1:T(8,128)(2,1)S(1)} %bitcast.12) | data formatting | bytes 8192
